TPU v7x, 512 devices: a whole 4x8x8 slice. The times are simulated.
512 devices in a mesh: sp: 32 (over z, x), tp: 16 (over y, core).
Axes of the slice: x: 4, y: 8, z: 8, core: 2. Of those that a mesh axis runs over, the one named last changes fastest.
Arguments:
- residual: bfloat16 [8192, 2048], P('sp', 'tp'), may hold values from -6 to 6
- queries: bfloat16 [8192, 1024], P('sp', 'tp'), may hold values from -5.5 to 5.5
- keys: bfloat16 [8192, 128], P('sp'), may hold values from -5.5 to 5.5
- values: bfloat16 [8192, 128], P('sp'), may hold values from -6 to 6
- documents: int32 [8192], P('sp'), may hold values from 0 to 15, never falling along the last dimension, each value on 1 to 1024 neighbouring positions
- sinks: float32 [16], P('tp'), may hold values from 1 to 6
- head_gain: float32 [1024], replicated, may hold values from 0.1 to 1.9
- out_weight: bfloat16 [1024, 2048], P(None, 'tp'), may hold values from -0.1875 to 0.1875
- norm_gain: float32 [2048], P('tp'), may hold values from 0.1 to 1.9
- norm_shift: float32 [2048], P('tp'), may hold values from -3 to 3
- routes: int32 [8192, 2], P('sp'), may hold values from 0 to 31, all different within a row; in each aligned block of 256 rows (0 to 255, 256 to 511, ...) at most 24 rows name the same one
- route_logits: float32 [8192, 2], P('sp'), may hold values from -150 to 150
- gate_weight: bfloat16 [32, 2048, 6144], P('sp', None, 'tp'), may hold values from -0.125 to 0.125
- up_weight: bfloat16 [32, 2048, 6144], P('sp', None, 'tp'), may hold values from -0.125 to 0.125
- down_weight: bfloat16 [32, 6144, 2048], P('sp', 'tp'), may hold values from -0.15625 to 0.15625
- final_gain: float32 [2048], P('tp'), may hold values from 0.1 to 1.9
- final_shift: float32 [2048], P('tp'), may hold values from -3 to 3
Outputs:
- layer_out: bfloat16 [8192, 2048], P('sp', 'tp')
Inputs may be any that keep to these rules, and one draw needn't show every extreme that they name: `documents`: document numbers never fall along the sequence; each document has at least one position and at most 1024, and some document has exactly 1024. `routes`: each row names 2 different experts. In each aligned block of 256 rows (the rows of one index of sp) no expert is named by more than 24 rows, a bound that some block reaches.
All inputs are finite; a program needn't handle non-finite values.
Results may differ from a plain program's by a relative error of at most 0.014.
Values may be sent and summed in bfloat16 or wider, within the bound.
A program may use at most 128 MiB of HBM per device.

v0:
```python
import jax
import jax.numpy as jnp
from jax import lax
from jax.sharding import PartitionSpec as P

D = 2048
QUERY_HEADS = 16
KEY_VALUE_HEADS = 2
HEAD_SIZE = 64
WINDOW_SIZE = 128
TOP = 2


DEEP_ALPHA = 8.0**0.25
NORM_EPS = 1e-05


def sent_to_all(value, axis):
    length = lax.axis_size(axis)
    return lax.all_to_all(
        jnp.broadcast_to(value[None], (length, *value.shape)), axis, 0, 0, tiled=True
    )


def over_copies(value, axis):
    return sent_to_all(value, axis).sum(axis=0)


def in_one(arrays, axis):
    line, at, gathered = (jnp.concatenate([a.reshape(-1) for a in arrays]), 0, [])
    total = over_copies(line, axis)
    for a in arrays:
        gathered.append(total[at : at + a.size].reshape(a.shape))
        at += a.size
    return tuple(gathered)


def shifted(block, axis, distance):
    devices = range(lax.axis_size(axis))
    route = [(i - distance, i) for i in devices if i - distance in devices]
    return lax.ppermute(block, axis, route)


def split_norm(total, gain, shift):
    totals = in_one((jnp.sum(total, axis=1), jnp.sum(total * total, axis=1)), "tp")
    center = totals[0] / D
    spread = totals[1] / D - center * center
    return (total - center[:, None]) * lax.rsqrt(spread + NORM_EPS)[:, None] * gain + shift


def expert_rows(arrived, gate_weight, up_weight, down_weight):
    sources, count, width = arrived.shape
    flat_rows = arrived.reshape(sources * count, width)
    gate = jnp.dot(flat_rows, gate_weight[0], preferred_element_type=jnp.float32)
    up_val = jnp.dot(flat_rows, up_weight[0], preferred_element_type=jnp.float32)
    middle = (jax.nn.silu(gate) * up_val).astype(jnp.bfloat16)
    share_out = jnp.dot(middle, down_weight[0], preferred_element_type=jnp.float32).astype(
        jnp.bfloat16
    )
    groups = lax.axis_size("tp")
    pieces = share_out.reshape(sources, count, groups, width // groups)
    traded = lax.all_to_all(pieces, "tp", split_axis=2, concat_axis=2, tiled=True)
    summed = jnp.sum(traded.astype(jnp.float32), axis=2)
    return lax.all_to_all(
        summed.astype(jnp.bfloat16), "sp", split_axis=0, concat_axis=0, tiled=True
    )


def pack_rows(source_rows, table, expert_count, capacity):
    padded = jnp.concatenate(
        [source_rows, jnp.zeros((1, source_rows.shape[1]), source_rows.dtype)], axis=0
    )
    return padded[table].reshape(expert_count, capacity, source_rows.shape[1])


def local(
    residual,
    queries,
    keys,
    values,
    documents,
    sinks,
    head_gain,
    out_weight,
    norm_gain,
    norm_shift,
    routes,
    route_logits,
    gate_weight,
    up_weight,
    down_weight,
    final_gain,
    final_shift,
):
    tokens = queries.shape[0]
    head_list = sinks.shape[0]
    tails = shifted(
        (
            keys[tokens - WINDOW_SIZE :],
            values[tokens - WINDOW_SIZE :],
            documents[tokens - WINDOW_SIZE :].astype(jnp.bfloat16),
        ),
        "sp",
        1,
    )
    offset = lax.axis_index("sp") * tokens
    shared_key_head = lax.axis_index("tp") * head_list // (QUERY_HEADS // KEY_VALUE_HEADS)
    all_keys = jnp.concatenate([tails[0], keys], axis=0)
    all_values = jnp.concatenate([tails[1], values], axis=0)
    all_docs = jnp.concatenate([tails[2].astype(jnp.int32), documents], axis=0)
    key_head = lax.dynamic_slice_in_dim(all_keys, shared_key_head * HEAD_SIZE, HEAD_SIZE, 1)
    value_head = lax.dynamic_slice_in_dim(all_values, shared_key_head * HEAD_SIZE, HEAD_SIZE, 1)
    query_heads = queries.reshape(tokens, head_list, HEAD_SIZE)
    scores = jnp.einsum(
        "qhd,kd->hqk", query_heads, key_head, preferred_element_type=jnp.float32
    ) * HEAD_SIZE ** (-0.5)
    query_pos = offset + jnp.arange(tokens, dtype=jnp.int32)
    key_pos = offset - WINDOW_SIZE + jnp.arange(tokens + WINDOW_SIZE, dtype=jnp.int32)
    distance = query_pos[:, None] - key_pos[None, :]
    allowed = (
        (distance >= 0)
        & (distance < WINDOW_SIZE)
        & (key_pos[None, :] >= 0)
        & (documents[:, None] == all_docs[None, :])
    )
    scores = jnp.where(allowed[None], scores, -jnp.inf)
    sink_col = sinks[:, None]
    top = jnp.maximum(jnp.max(scores, axis=2), sink_col)
    expd = jnp.exp(scores - top[..., None])
    probs = (expd / (jnp.sum(expd, axis=2) + jnp.exp(sink_col - top))[..., None]).astype(
        jnp.bfloat16
    )
    attended = jnp.einsum("hqk,kd->qhd", probs, value_head, preferred_element_type=jnp.float32)
    attended = attended.astype(jnp.bfloat16).reshape(tokens, head_list * HEAD_SIZE)
    all_heads = lax.all_gather(attended, "tp", axis=1, tiled=True).astype(jnp.float32)
    scaled = (
        all_heads
        * lax.rsqrt(jnp.mean(all_heads * all_heads, axis=1, keepdims=True) + NORM_EPS)
        * head_gain
    ).astype(jnp.bfloat16)
    mix = jnp.dot(scaled, out_weight, preferred_element_type=jnp.float32)
    first = DEEP_ALPHA * residual.astype(jnp.float32) + mix
    hidden = split_norm(first, norm_gain, norm_shift)
    hidden_rows = hidden.astype(jnp.bfloat16)
    expert_count = lax.axis_size("sp")
    capacity = 3 * tokens * TOP // (2 * expert_count)
    flat = routes.reshape(-1)
    onehot = (flat[:, None] == jnp.arange(expert_count, dtype=jnp.int32)[None, :]).astype(jnp.int32)
    rank = jnp.sum(jnp.cumsum(onehot, axis=0) * onehot, axis=1) - 1
    target = flat * capacity + rank
    owner = jnp.arange(tokens * TOP, dtype=jnp.int32) // TOP
    table = jnp.full((expert_count * capacity,), tokens, jnp.int32).at[target].set(owner)
    outgoing = pack_rows(hidden_rows, table, expert_count, capacity)
    joined = lax.all_gather(
        lax.all_to_all(outgoing, "sp", split_axis=0, concat_axis=0, tiled=True),
        "tp",
        axis=2,
        tiled=True,
    )
    returned = expert_rows(joined, gate_weight, up_weight, down_weight)
    picked = (
        returned.reshape(expert_count * capacity, -1)[target]
        .reshape(tokens, TOP, -1)
        .astype(jnp.float32)
    )
    share = jax.nn.softmax(route_logits, axis=-1)
    moe = jnp.sum(share[:, :, None] * picked, axis=1)
    second = DEEP_ALPHA * hidden + moe
    return split_norm(second, final_gain, final_shift).astype(jnp.bfloat16)


def solution(mesh):
    return jax.shard_map(
        local,
        mesh=mesh,
        in_specs=(
            P("sp", "tp"),
            P("sp", "tp"),
            P("sp", None),
            P("sp", None),
            P("sp"),
            P("tp"),
            P(),
            P(None, "tp"),
            P("tp"),
            P("tp"),
            P("sp", None),
            P("sp", None),
            P("sp", None, "tp"),
            P("sp", None, "tp"),
            P("sp", "tp", None),
            P("tp"),
            P("tp"),
        ),
        out_specs=P("sp", "tp"),
        check_vma=False,
    )
```

profile of v0, /device:TPU:1, one launch (start us, length us, event | category | flops | bytes accessed | tf_op | source)
XLA Modules:
  0.0 268.2 jit_solution(7688286295900288744)
XLA Ops:
  6.5 0.9 slice.30
  7.4 3.9 %collective-permute-start.2 = (bf16[128,128]{1,0:T(8,128)(2,1)S(1)}, bf16[128,128]{1,0:T(8,128)(2,1)S(1)}, u32[]{:S(2)}, u32[]{:S(2)}) collective-permute-start(bf16[128,128]{1,0:T(8,128)(2,1)S(1)} %slice.30), channel_id=1, source_target_pairs={{0,16},{16,32},{32,48},{48,64},{64,80},{80,96},{96,112},{112,128},... | collective-permute-start | bytes 98312 | tf_op jit(solution)/shard_map/ppermute | solution.py:41
  11.4 0.7 convert.5
  12.0 3.1 %collective-permute-start.1 = (bf16[128]{0:T(256)(128)(2,1)S(1)}, bf16[128]{0:T(256)(128)(2,1)S(1)}, u32[]{:S(2)}, u32[]{:S(2)}) collective-permute-start(bf16[128]{0:T(256)(128)(2,1)S(1)} %slice.29), channel_id=1, source_target_pairs={{0,16},{16,32},{32,48},{48,64},{64,80},{80,96},{96,112},{112,128},... | collective-permute-start | bytes 776 | tf_op jit(solution)/shard_map/ppermute | solution.py:41
  15.2 0.8 slice.28
  15.9 2.8 %collective-permute-start = (bf16[128,128]{1,0:T(8,128)(2,1)S(1)}, bf16[128,128]{1,0:T(8,128)(2,1)S(1)}, u32[]{:S(2)}, u32[]{:S(2)}) collective-permute-start(bf16[128,128]{1,0:T(8,128)(2,1)S(1)} %slice.28), channel_id=1, source_target_pairs={{0,16},{16,32},{32,48},{48,64},{64,80},{80,96},{96,112},{112,128},... | collective-permute-start | bytes 98312 | tf_op jit(solution)/shard_map/ppermute | solution.py:41
  18.8 0.8 copy.39
  19.6 0.1 eq.52
  19.8 0.1 eq.48
  19.9 0.7 broadcast_multiply_fusion
  20.6 1.2 reduce-window.6
  21.8 0.2 slice_reduce_fusion
  22.0 0.1 fusion.39
  22.2 0.1 copy.38
  22.3 0.1 mul.144
  22.5 2.4 scatter_custom_fusion
  25.6 0.7 pad_add_fusion
  26.3 1.2 fusion.55
  27.5 0.0 copy-start.8
  27.5 0.1 fusion.28
  27.7 0.3 fusion.14
  28.0 20.4 %all-gather = bf16[256,1,1024]{0,2,1:T(8,128)(2,1)S(1)} all-gather(bf16[256,1,64]{0,2,1:T(8,128)(2,1)S(1)} %fusion.14), channel_id=2, replica_groups=mesh['sp'=32,'tp'=16] {'tp'}, dimensions={2}, use_global_device_ids=true | all-gather | bytes 557056 | tf_op jit(solution)/shard_map/all_gather | solution.py:135
  48.3 0.2 fusion.15
  48.6 0.7 fusion.54
  49.2 0.6 broadcast_in_dim.13
  49.9 4.5 %all-to-all-start = ((f32[16,1,512]{2,1,0:T(1,128)}), f32[16,1,512]{2,1,0:T(1,128)S(1)}, u32[]{:S(2)}, u32[]{:S(2)}) async-start(f32[16,1,512]{2,1,0:T(1,128)} %broadcast_in_dim.13), calls=%async_computation | async-start | bytes 65536 | tf_op jit(solution)/shard_map/all_to_all | solution.py:20
  54.4 0.0 all-gather.3.cloned.1.call-start
  54.4 7.3 %all-to-all-done = f32[16,1,512]{2,1,0:T(1,128)S(1)} async-done(((f32[16,1,512]{2,1,0:T(1,128)}), f32[16,1,512]{2,1,0:T(1,128)S(1)}, u32[]{:S(2)}, u32[]{:S(2)}) %all-to-all-start) | async-done | bytes 32800 | tf_op jit(solution)/shard_map/all_to_all | solution.py:20
  61.8 0.1 fusion.31
  62.0 1.9 gather_fusion
  63.9 23.3 %all_to_all.27 = bf16[32,24,128]{2,1,0:T(8,128)(2,1)} all-to-all(bf16[32,24,128]{2,1,0:T(8,128)(2,1)S(1)} %bitcast.72), channel_id=1, replica_groups=mesh['sp'=32,'tp'=16] {'sp'}, dimensions={0} | all-to-all | bytes 393216 | tf_op jit(solution)/shard_map/all_to_all | solution.py:155
  87.2 0.0 all-gather.3.cloned.1.call-update
  87.2 39.9 %all-gather.3.cloned.1.call-done = bf16[32,24,2048]{2,1,0:T(8,128)(2,1)} async-done(((bf16[32,24,128]{2,1,0:T(8,128)(2,1)}), bf16[32,24,2048]{2,1,0:T(8,128)(2,1)}) %all-gather.3.cloned.1.call-update) | async-done | bytes 3145744 | tf_op jit(solution)/shard_map/all_gather | solution.py:154
  127.1 5.3 %fusion.4 = f32[768,384]{1,0:T(8,128)} fusion(bf16[768,2048]{1,0:T(8,128)(2,1)} %bitcast.77, bf16[1,2048,384]{2,1,0:T(8,128)(2,1)} %param.29), kind=kOutput, calls=%fused_computation.8 | convolution fusion | flops 1207959552 | bytes 5898240 | tf_op jit(solution)/shard_map/dot_general | solution.py:54
  132.4 7.4 %fusion = bf16[96,8,16,128]{3,1,2,0:T(8,128)(2,1)} fusion(bf16[1,384,2048]{2,1,0:T(8,128)(2,1)S(1)} %copy-done, bf16[768,2048]{1,0:T(8,128)(2,1)} %bitcast.78, bf16[1,2048,384]{2,1,0:T(8,128)(2,1)S(1)} %copy-done.7, f32[768,384]{1,0:T(8,128)} %fusion.4), kind=kOutput, calls=%fused_computation.4 | convolution fusion | flops 2419261440 | bytes 10616832 | tf_op jit(solution)/shard_map/dot_general | solution.py:57
  139.7 2.9 %copy.51 = bf16[96,8,16,128]{3,2,1,0:T(8,128)(2,1)S(1)} copy(bf16[96,8,16,128]{3,1,2,0:T(8,128)(2,1)} %fusion) | data formatting | bytes 6291456
  142.6 2.5 copy.42
  145.2 4.6 %all-to-all-start.2 = ((bf16[32,24,16,128]{3,1,0,2:T(8,128)(2,1)}), bf16[32,24,16,128]{3,1,0,2:T(8,128)(2,1)}, u32[]{:S(2)}, u32[]{:S(2)}) async-start(bf16[32,24,16,128]{3,1,0,2:T(8,128)(2,1)} %copy.42), calls=%async_computation.2 | async-start | bytes 6291456 | tf_op jit(solution)/shard_map/all_to_all | solution.py:62
  149.8 71.1 %all-to-all-done.2 = bf16[32,24,16,128]{3,1,0,2:T(8,128)(2,1)} async-done(((bf16[32,24,16,128]{3,1,0,2:T(8,128)(2,1)}), bf16[32,24,16,128]{3,1,0,2:T(8,128)(2,1)}, u32[]{:S(2)}, u32[]{:S(2)}) %all-to-all-start.2) | async-done | bytes 3145760 | tf_op jit(solution)/shard_map/all_to_all | solution.py:62
  220.9 3.1 %reduce_sum.118 = bf16[32,24,128]{2,1,0:T(8,128)(2,1)} reduce(bf16[32,24,16,128]{3,1,0,2:T(8,128)(2,1)} %all-to-all-done.2, bf16[]{:T(256)} %constant.87.clone.1), dimensions={2}, to_apply=%region_12.13 | reduce | flops 1474560 | bytes 3342338 | tf_op jit(solution)/shard_map/reduce_sum | solution.py:63
  223.9 9.7 %all-to-all-start.3 = ((bf16[32,24,128]{2,1,0:T(8,128)(2,1)}), bf16[32,24,128]{2,1,0:T(8,128)(2,1)S(1)}, u32[]{:S(2)}, u32[]{:S(2)}) async-start(bf16[32,24,128]{2,1,0:T(8,128)(2,1)} %reduce_sum.118), calls=%async_computation.3 | async-start | bytes 393216 | tf_op jit(solution)/shard_map/all_to_all | solution.py:64
  233.7 0.1 copy.37
  233.9 9.7 %all-to-all-done.3 = bf16[32,24,128]{2,1,0:T(8,128)(2,1)S(1)} async-done(((bf16[32,24,128]{2,1,0:T(8,128)(2,1)}), bf16[32,24,128]{2,1,0:T(8,128)(2,1)S(1)}, u32[]{:S(2)}, u32[]{:S(2)}) %all-to-all-start.3) | async-done | bytes 196640 | tf_op jit(solution)/shard_map/all_to_all | solution.py:64
  243.6 1.3 gather_fusion.1
  244.9 0.4 fusion.29
  245.3 0.3 fusion.53
  245.6 14.9 %all_to_all.28 = f32[16,1,512]{2,1,0:T(1,128)S(1)} all-to-all(f32[16,1,512]{2,1,0:T(1,128)S(1)} %broadcast_in_dim.16), channel_id=1, replica_groups=mesh['sp'=32,'tp'=16] {'tp'}, dimensions={0} | all-to-all | bytes 65536 | tf_op jit(solution)/shard_map/all_to_all | solution.py:20
  260.6 0.8 add_convert_fusion
  (52 shorter events, 0.4 us)
Async XLA Ops:
  6.5 125.8 %copy-start = (bf16[1,384,2048]{2,1,0:T(8,128)(2,1)S(1)}, bf16[1,384,2048]{2,1,0:T(8,128)(2,1)}, u32[]{:S(2)}) copy-start(bf16[1,384,2048]{2,1,0:T(8,128)(2,1)} %param.31) | copy-start | bytes 4718596
  6.5 21.1 %copy-start.2 = (bf16[256,128]{1,0:T(8,128)(2,1)S(1)}, bf16[256,128]{1,0:T(8,128)(2,1)}, u32[]{:S(2)}) copy-start(bf16[256,128]{1,0:T(8,128)(2,1)} %param.20) | copy-start | bytes 196612
  7.4 18.9 %collective-permute-start.2 = (bf16[128,128]{1,0:T(8,128)(2,1)S(1)}, bf16[128,128]{1,0:T(8,128)(2,1)S(1)}, u32[]{:S(2)}, u32[]{:S(2)}) collective-permute-start(bf16[128,128]{1,0:T(8,128)(2,1)S(1)} %slice.30), channel_id=1, source_target_pairs={{0,16},{16,32},{32,48},{48,64},{64,80},{80,96},{96,112},{112,128},... | collective-permute-start | bytes 98312 | tf_op jit(solution)/shard_map/ppermute | solution.py:41
  12.0 13.5 %collective-permute-start.1 = (bf16[128]{0:T(256)(128)(2,1)S(1)}, bf16[128]{0:T(256)(128)(2,1)S(1)}, u32[]{:S(2)}, u32[]{:S(2)}) collective-permute-start(bf16[128]{0:T(256)(128)(2,1)S(1)} %slice.29), channel_id=1, source_target_pairs={{0,16},{16,32},{32,48},{48,64},{64,80},{80,96},{96,112},{112,128},... | collective-permute-start | bytes 776 | tf_op jit(solution)/shard_map/ppermute | solution.py:41
  15.9 11.7 %collective-permute-start = (bf16[128,128]{1,0:T(8,128)(2,1)S(1)}, bf16[128,128]{1,0:T(8,128)(2,1)S(1)}, u32[]{:S(2)}, u32[]{:S(2)}) collective-permute-start(bf16[128,128]{1,0:T(8,128)(2,1)S(1)} %slice.28), channel_id=1, source_target_pairs={{0,16},{16,32},{32,48},{48,64},{64,80},{80,96},{96,112},{112,128},... | collective-permute-start | bytes 98312 | tf_op jit(solution)/shard_map/ppermute | solution.py:41
  27.5 21.0 %copy-start.8 = (bf16[1024,128]{1,0:T(8,128)(2,1)S(1)}, bf16[1024,128]{1,0:T(8,128)(2,1)}, u32[]{:S(2)}) copy-start(bf16[1024,128]{1,0:T(8,128)(2,1)} %param.24) | copy-start | bytes 786436
  27.5 21.0 %copy-start.9 = (bf16[256,128]{1,0:T(8,128)(2,1)S(1)}, bf16[256,128]{1,0:T(8,128)(2,1)}, u32[]{:S(2)}) copy-start(bf16[256,128]{1,0:T(8,128)(2,1)} %param.17) | copy-start | bytes 196612
  27.5 21.0 %copy-start.10 = (f32[1024]{0:T(1024)S(1)}, f32[1024]{0:T(1024)}, u32[]{:S(2)}) copy-start(f32[1024]{0:T(1024)} %param.23) | copy-start | bytes 12292
  27.9 33.9 %copy-start.3 = (f32[128]{0:T(128)S(1)}, f32[128]{0:T(128)}, u32[]{:S(2)}) copy-start(f32[128]{0:T(128)} %param.26) | copy-start | bytes 1540
  28.0 33.8 %copy-start.4 = (f32[128]{0:T(128)S(1)}, f32[128]{0:T(128)}, u32[]{:S(2)}) copy-start(f32[128]{0:T(128)} %param.25) | copy-start | bytes 1540
  49.9 11.9 %all-to-all-start = ((f32[16,1,512]{2,1,0:T(1,128)}), f32[16,1,512]{2,1,0:T(1,128)S(1)}, u32[]{:S(2)}, u32[]{:S(2)}) async-start(f32[16,1,512]{2,1,0:T(1,128)} %broadcast_in_dim.13), calls=%async_computation | async-start | bytes 65536 | tf_op jit(solution)/shard_map/all_to_all | solution.py:20
  54.4 72.7 %all-gather.3.cloned.1.call-start = ((), (), s32[]{:S(2)}) async-start(), calls=%async_computation.5 | async-start | bytes 3342336 | tf_op jit(solution)/shard_map/all_gather | solution.py:154
  127.1 5.3 %copy-start.7 = (bf16[1,2048,384]{2,1,0:T(8,128)(2,1)S(1)}, bf16[1,2048,384]{2,1,0:T(8,128)(2,1)}, u32[]{:S(2)}) copy-start(bf16[1,2048,384]{2,1,0:T(8,128)(2,1)} %param.30) | copy-start | bytes 4718596
  145.2 4.6 %copy-start.1 = (f32[256,2]{0,1:T(2,128)S(1)}, f32[256,2]{0,1:T(2,128)}, u32[]{:S(2)}) copy-start(f32[256,2]{0,1:T(2,128)} %param.28) | copy-start | bytes 6148
  145.2 75.7 %all-to-all-start.2 = ((bf16[32,24,16,128]{3,1,0,2:T(8,128)(2,1)}), bf16[32,24,16,128]{3,1,0,2:T(8,128)(2,1)}, u32[]{:S(2)}, u32[]{:S(2)}) async-start(bf16[32,24,16,128]{3,1,0,2:T(8,128)(2,1)} %copy.42), calls=%async_computation.2 | async-start | bytes 6291456 | tf_op jit(solution)/shard_map/all_to_all | solution.py:62
  223.9 36.6 %copy-start.5 = (f32[128]{0:T(128)S(1)}, f32[128]{0:T(128)}, u32[]{:S(2)}) copy-start(f32[128]{0:T(128)} %param.33) | copy-start | bytes 1540
  223.9 36.6 %copy-start.6 = (f32[128]{0:T(128)S(1)}, f32[128]{0:T(128)}, u32[]{:S(2)}) copy-start(f32[128]{0:T(128)} %param.32) | copy-start | bytes 1540
  223.9 19.6 %all-to-all-start.3 = ((bf16[32,24,128]{2,1,0:T(8,128)(2,1)}), bf16[32,24,128]{2,1,0:T(8,128)(2,1)S(1)}, u32[]{:S(2)}, u32[]{:S(2)}) async-start(bf16[32,24,128]{2,1,0:T(8,128)(2,1)} %reduce_sum.118), calls=%async_computation.3 | async-start | bytes 393216 | tf_op jit(solution)/shard_map/all_to_all | solution.py:64
Sparse Core Ops, SparseCore 0:
  87.3 39.7 all-gather.2
where the time goes:
time: 269 us; the launch traced here: 268 us
  waiting for transfers between devices  128 us (48%)
  blocking collectives  58.5 us (22%)
  starting transfers between devices  28.7 us (11%)
  local copies, waits for them, and re-layouts  15.2 us (6%)
  matrix products  14.8 us (6%)
  between operations  14.4 us (5%)
  other arithmetic  8.54 us (3%)
    all_to_all x1, waiting for transfers between devices, expert_rows(): lax.all_to_all(pieces, 'tp', split_axis=2, concat_axis=2, tiled=True)  71.1 us
    all_gather x1, waiting for transfers between devices, local(): lax.all_gather(lax.all_to_all(outgoing, 'sp', split_axis=0, concat_axis=0...  39.9 us
    all_to_all x1, blocking collectives, local(): lax.all_to_all(outgoing, 'sp', split_axis=0, concat_axis=0, tiled=True)  23.3 us
    all_gather x1, blocking collectives, local(): lax.all_gather(attended, 'tp', axis=1, tiled=True).astype(jnp.float32)  20.4 us
    all_to_all x1, blocking collectives, sent_to_all(): lax.all_to_all(jnp.broadcast_to(value[None], (length, *value.shape)), axi...  14.9 us
    ppermute x3, starting transfers between devices, shifted(): return lax.ppermute(block, axis, route)  9.84 us
    all_to_all x1, starting transfers between devices, expert_rows(): lax.all_to_all(summed.astype(jnp.bfloat16), 'sp', split_axis=0, concat_ax...  9.73 us
    all_to_all x1, waiting for transfers between devices, expert_rows(): lax.all_to_all(summed.astype(jnp.bfloat16), 'sp', split_axis=0, concat_ax...  9.68 us
  transfers between devices with their start and end apart: 7, of which 4 were waited for; matrix products, arithmetic and copies ran while one was open for 4% of the time, Pallas kernels for 0%

commit v1 on v0

v1 whole, which is shorter than its diff:
```python
import jax
import jax.numpy as jnp
from jax import lax
from jax.experimental import pallas as pl
from jax.experimental.pallas import tpu as pltpu
from jax.sharding import PartitionSpec as P

D = 2048
HEAD = 64
WINDOW = 128
TOK = 256
CAP = 24
SP = 32
TP = 16
NY = 8
COLS = D // TP
ROWS = SP * CAP
HALF = ROWS // 2
FFB = 384
ALPHA = 8.0**0.25
EPS = 1e-05
MESH = pl.DeviceIdType.MESH
BF = jnp.bfloat16
F32 = jnp.float32

RIGHT = [(0, 0), (0, 1), (1, 0), (1, 1), (2, 0), (2, 1), (3, 0)]
LEFT = [(0, 1), (0, 0), (1, 1), (1, 0), (2, 1), (2, 0), (3, 1)]
DESTS = [4, 3, 5, 2, 6, 1, 7, 0]
SUM_RIGHT = [(0, 0), (1, 1), (1, 0), (3, 1), (3, 0), (5, 1), (5, 0)]
SUM_LEFT = [(0, 1), (2, 0), (2, 1), (4, 0), (4, 1), (6, 0), (6, 1)]


def dot(a, b):
    return lax.dot_general(a, b, (((1,), (0,)), ((), ())), preferred_element_type=F32)


def dot_nt(a, b):
    return lax.dot_general(a, b, (((1,), (1,)), ((), ())), preferred_element_type=F32)


def column(row):
    return jnp.transpose(jnp.broadcast_to(row, (128, 128)))


def twice(a):
    return jnp.concatenate([a, a], axis=1)


def kernel(
    residual, queries, keys, values, docs, sinks, head_gain, out_weight, norm_gain, norm_shift,
    routes, logits, final_gain, final_shift, gate_hbm, up_hbm, down_hbm,
    out,
    wgu, wd, tail_k, tail_v, tail_d, wot, res, vt, select, mix_hi, mix_lo,
    att, stat1, stat2, hid, going, came, grid, acc, mid, mine, sib_out, sib_in,
    right_out, right_in, left_out, left_in, back_out, back_in,
    w_sem, tail_sem, a_send, a_recv, as_send, as_recv, s_send, s_recv, s2_send, s2_recv,
    d_send, d_recv, gr_send, gr_recv, gl_send, gl_recv, gs_send, gs_recv,
    rs_send, rs_recv, rr_send, rr_recv, rl_send, rl_recv, b_send, b_recv, own_sem,
):
    sp = lax.axis_index("sp")
    tp = lax.axis_index("tp")
    y = lax.div(tp, 2)
    c = lax.rem(tp, 2)
    sibling = {"tp": y * 2 + 1 - c}

    def chip(distance):
        return lax.rem(y + distance, NY)

    def on_y(distance):
        return {"tp": chip(distance) * 2 + c}

    def send(src, dst, send_sem, recv_sem, device):
        pltpu.make_async_remote_copy(
            src_ref=src, dst_ref=dst, send_sem=send_sem, recv_sem=recv_sem,
            device_id=device, device_id_type=MESH,
        ).start()

    def arrived(dst, send_sem, recv_sem, device):
        pltpu.make_async_remote_copy(
            src_ref=dst, dst_ref=dst, send_sem=send_sem, recv_sem=recv_sem,
            device_id=device, device_id_type=MESH,
        ).wait_recv()

    def left_here(src, send_sem, recv_sem, device):
        pltpu.make_async_remote_copy(
            src_ref=src, dst_ref=src, send_sem=send_sem, recv_sem=recv_sem,
            device_id=device, device_id_type=MESH,
        ).wait_send()

    w_copies = [
        pltpu.make_async_copy(gate_hbm.at[0], wgu.at[:, 0:FFB], w_sem.at[0]),
        pltpu.make_async_copy(up_hbm.at[0], wgu.at[:, FFB : 2 * FFB], w_sem.at[1]),
    ]
    for d in range(NY):
        for part in range(2):
            block = 2 * d + (c if part == 0 else 1 - c)
            w_copies.append(
                pltpu.make_async_copy(
                    down_hbm.at[0, :, pl.ds(pl.multiple_of(block * 128, 128), 128)],
                    wd.at[d, :, 128 * part : 128 * part + 128],
                    w_sem.at[2 + 2 * d + part],
                )
            )
    for copy in w_copies:
        copy.start()

    barrier = pltpu.get_barrier_semaphore()

    def greet_tp(k, carry):
        pl.semaphore_signal(barrier, inc=1, device_id={"tp": lax.rem(tp + k, TP)}, device_id_type=MESH)
        return carry

    def greet_sp(k, carry):
        pl.semaphore_signal(barrier, inc=1, device_id={"sp": lax.rem(sp + k, SP)}, device_id_type=MESH)
        return carry

    lax.fori_loop(1, TP, greet_tp, 0)
    lax.fori_loop(1, SP, greet_sp, 0)

    upper = tp >= TP // 2
    vt[:, WINDOW:] = jnp.transpose(values[...].astype(F32)).astype(BF)
    qt = queries[...]
    zero_q = jnp.zeros_like(qt)
    q_wide = jnp.concatenate([jnp.where(upper, zero_q, qt), jnp.where(upper, qt, zero_q)], axis=0)
    doc_row = docs[...].astype(F32)
    sink = sinks[0, 0]

    def attend(key_rows, v_cols, key_docs, begin):
        score = dot(key_rows, q_wide[:, begin : begin + 128]) * HEAD ** (-0.5)
        ahead = (
            WINDOW
            + lax.broadcasted_iota(jnp.int32, (256, 128), 1)
            - lax.broadcasted_iota(jnp.int32, (256, 128), 0)
        )
        allowed = (ahead >= 0) & (ahead < WINDOW) & (key_docs == doc_row[:, begin : begin + 128])
        score = jnp.where(allowed, score, -1e30)
        top = jnp.maximum(jnp.max(score, axis=0, keepdims=True), sink)
        e = jnp.exp(score - top)
        total = jnp.sum(e, axis=0, keepdims=True) + jnp.exp(sink - top)
        probs = (e * (1.0 / total)).astype(BF)
        wide = dot(v_cols, probs)
        return jnp.where(upper, wide[HEAD:, :], wide[:HEAD, :]).astype(BF)

    docs0 = column(doc_row[:, 0:128])
    docs1 = column(doc_row[:, 128:256])
    att[tp, :, 128:256] = attend(keys[...], vt[:, 128:384], jnp.concatenate([docs0, docs1], axis=0), 128)

    pl.semaphore_wait(barrier, TP - 1 + SP - 1)

    after = {"sp": lax.rem(sp + 1, SP)}
    send(keys.at[128:256], tail_k, tail_sem.at[0], tail_sem.at[3], after)
    send(values.at[128:256], tail_v, tail_sem.at[1], tail_sem.at[4], after)
    send(docs.at[:, 128:256], tail_d, tail_sem.at[2], tail_sem.at[5], after)

    wot[...] = (jnp.transpose(out_weight[...].astype(F32)) * head_gain[...]).astype(BF)
    res[...] = ALPHA * jnp.transpose(residual[...].astype(F32))

    arrived(tail_k, tail_sem.at[0], tail_sem.at[3], after)
    arrived(tail_v, tail_sem.at[1], tail_sem.at[4], after)
    arrived(tail_d, tail_sem.at[2], tail_sem.at[5], after)
    vt[:, 0:WINDOW] = jnp.transpose(tail_v[...].astype(F32)).astype(BF)
    before_docs = jnp.where(sp > 0, tail_d[...].astype(F32), -1.0)
    att[tp, :, 0:128] = attend(
        jnp.concatenate([tail_k[...], keys[0:128, :]], axis=0),
        vt[:, 0:256],
        jnp.concatenate([column(before_docs), docs0], axis=0),
        0,
    )

    send(att.at[tp], att.at[tp], as_send.at[0], as_recv.at[0], sibling)
    for k in (4, 3, 5, 2, 6, 1, 7):
        send(att.at[tp], att.at[tp], a_send.at[k], a_recv.at[k], on_y(k))

    r0, r1 = routes[0:1, :], routes[1:2, :]
    experts = lax.broadcasted_iota(jnp.int32, (SP, TOK), 0)
    first_hit, second_hit = r0 == experts, r1 == experts
    named = jnp.where(first_hit | second_hit, 1.0, 0.0)
    earlier = jnp.where(
        lax.broadcasted_iota(jnp.int32, (TOK, TOK), 0) < lax.broadcasted_iota(jnp.int32, (TOK, TOK), 1), 1.0, 0.0
    ).astype(BF)
    place = jnp.where(named > 0.0, dot(named.astype(BF), earlier), -1.0)
    l0, l1 = logits[0:1, :], logits[1:2, :]
    l_top = jnp.maximum(l0, l1)
    e0, e1 = jnp.exp(l0 - l_top), jnp.exp(l1 - l_top)
    per = 1.0 / (e0 + e1)
    share = jnp.where(first_hit, e0 * per, jnp.where(second_hit, e1 * per, 0.0))
    slots = lax.broadcasted_iota(jnp.int32, (CAP, TOK), 0).astype(F32)
    for group in range(4):
        hits, weights = [], []
        for e in range(8 * group, 8 * group + 8):
            hit = place[e : e + 1, :] == slots
            hits.append(jnp.where(hit, 1.0, 0.0))
            weights.append(jnp.where(hit, share[e : e + 1, :], 0.0))
        rows = pl.ds(group * 8 * CAP, 8 * CAP)
        weight = jnp.concatenate(weights, axis=0)
        high = weight.astype(BF)
        select[rows, :] = jnp.concatenate(hits, axis=0).astype(BF)
        mix_hi[rows, :] = high
        mix_lo[rows, :] = (weight - high.astype(F32)).astype(BF)
    gain1, shift1 = twice(column(norm_gain[...])), twice(column(norm_shift[...]))

    for k in (1, 7, 2, 6, 3, 5, 4):
        block = att.at[chip(NY - k) * 2 + c]
        arrived(block, a_send.at[k], a_recv.at[k], on_y(k))
        send(block, block, as_send.at[k], as_recv.at[k], sibling)
    for k in range(NY):
        arrived(att.at[chip(NY - k) * 2 + 1 - c], as_send.at[k], as_recv.at[k], sibling)

    heads = att[...].reshape(TP * HEAD, TOK)
    wide = heads.astype(F32)
    scale = lax.rsqrt(jnp.sum(wide * wide, axis=0, keepdims=True) * (1.0 / (TP * HEAD)) + EPS)
    first = res[...] + dot(wot[...], heads) * scale

    def totals(value, stat, send_sem, recv_sem):
        stat[tp] = jnp.concatenate(
            [jnp.sum(value, axis=0, keepdims=True), jnp.sum(value * value, axis=0, keepdims=True)], axis=0
        )

        def tell(k, carry):
            send(stat.at[tp], stat.at[tp], send_sem.at[k], recv_sem.at[k], {"tp": lax.rem(tp + k, TP)})
            return carry

        def hear(k, carry):
            arrived(stat.at[lax.rem(tp + TP - k, TP)], send_sem.at[k], recv_sem.at[k], {"tp": lax.rem(tp + k, TP)})
            return carry

        lax.fori_loop(1, TP, tell, 0)
        lax.fori_loop(1, TP, hear, 0)
        total = jnp.sum(stat[...], axis=0)
        center = total[0:1] * (1.0 / D)
        spread = total[1:2] * (1.0 / D) - center * center
        return center, lax.rsqrt(spread + EPS)

    center, scale = totals(first, stat1, s_send, s_recv)
    hidden = (first - center) * scale * gain1 + shift1
    hid[...] = hidden

    packed = dot_nt(select[...], hidden.astype(BF))
    going[...] = packed.reshape(SP, CAP, COLS).astype(BF)
    own = pltpu.make_async_copy(going.at[sp], came.at[sp], own_sem.at[0])
    own.start()

    def out_go(k, carry):
        to = lax.rem(sp + k, SP)
        send(going.at[to], came.at[sp], d_send.at[k], d_recv.at[k], {"sp": to})
        return carry

    def out_come(k, carry):
        source = lax.rem(sp + SP - k, SP)
        arrived(came.at[source], d_send.at[k], d_recv.at[k], {"sp": lax.rem(sp + k, SP)})
        return carry

    lax.fori_loop(1, SP, out_go, 0)
    w_copies[0].wait()
    w_copies[1].wait()
    lax.fori_loop(1, SP, out_come, 0)
    own.wait()

    for half in range(2):
        block = came[16 * half : 16 * half + 16].astype(F32).reshape(HALF, COLS)
        grid[tp, half] = block.astype(BF)

    def piece(owner, half, core):
        return grid.at[chip(owner) * 2 + core, half]

    def ring_send(m, lanes):
        hops, half = lanes[m]
        if lanes is RIGHT:
            p = piece(NY - hops, half, c)
            send(p, p, gr_send.at[m], gr_recv.at[m], on_y(1))
        else:
            p = piece(hops, half, c)
            send(p, p, gl_send.at[m], gl_recv.at[m], on_y(NY - 1))

    def share_send(index, p):
        send(p, p, gs_send.at[index], gs_recv.at[index], sibling)

    for m in range(2):
        ring_send(m, RIGHT)
        ring_send(m, LEFT)
    for half in range(2):
        share_send(half, piece(0, half, c))

    def multiply(owner, half, fresh):
        at = chip(owner)
        both = jnp.concatenate([grid[at * 2, half], grid[at * 2 + 1, half]], axis=1)
        product = dot(both, wgu[pl.ds(pl.multiple_of(at * 256, 256), 256), :])
        if fresh:
            acc[half] = product
        else:
            acc[half] += product

    for half in range(2):
        arrived(piece(0, half, 1 - c), gs_send.at[half], gs_recv.at[half], sibling)
        multiply(0, half, True)
    waiting = []
    for m in range(7):
        now = []
        for lanes in (RIGHT, LEFT):
            hops, half = lanes[m]
            right = lanes is RIGHT
            owner = NY - 1 - hops if right else hops + 1
            p = piece(owner, half, c)
            s, r = (gr_send, gr_recv) if right else (gl_send, gl_recv)
            arrived(p, s.at[m], r.at[m], on_y(1 if right else NY - 1))
            if m + 2 < 7:
                ring_send(m + 2, lanes)
            index = 2 + 2 * m + (0 if right else 1)
            share_send(index, p)
            now.append((owner, half, index))
        for owner, half, index in waiting:
            arrived(piece(owner, half, 1 - c), gs_send.at[index], gs_recv.at[index], sibling)
            multiply(owner, half, False)
        waiting = now
    for owner, half, index in waiting:
        arrived(piece(owner, half, 1 - c), gs_send.at[index], gs_recv.at[index], sibling)
        multiply(owner, half, False)
    for copy in w_copies[2:]:
        copy.wait()
    for half in range(2):
        gate, up = acc[half, :, 0:FFB], acc[half, :, FFB:]
        mid[half] = (gate / (1.0 + jnp.exp(-gate)) * up).astype(BF)

    def partials(i):
        for half in range(2):
            product = dot(mid[half], wd[chip(DESTS[i])])
            mine[i, half] = product[:, 0:COLS]
            sib_out[i, half] = product[:, COLS:].astype(BF)
        send(sib_out.at[i], sib_in.at[i], rs_send.at[i], rs_recv.at[i], sibling)

    def paired(i):
        arrived(sib_in.at[i], rs_send.at[i], rs_recv.at[i], sibling)

    def summed(i, half):
        return mine[i, half] + sib_in[i, half].astype(F32)

    def pass_on(m):
        for lanes, o, n, s, r, d in (
            (SUM_RIGHT, right_out, right_in, rr_send, rr_recv, 1),
            (SUM_LEFT, left_out, left_in, rl_send, rl_recv, NY - 1),
        ):
            i, half = lanes[m]
            value = summed(i, half)
            if m >= 2:
                arrived(n.at[m - 2], s.at[m - 2], r.at[m - 2], on_y(d))
                value = value + n[m - 2].astype(F32)
            o[m] = value.astype(BF)
            send(o.at[m], n.at[m], s.at[m], r.at[m], on_y(d))

    partials(0)
    partials(1)
    partials(2)
    paired(0)
    pass_on(0)
    paired(1)
    paired(2)
    pass_on(1)
    partials(3)
    partials(4)
    pass_on(2)
    paired(3)
    paired(4)
    pass_on(3)
    partials(5)
    partials(6)
    pass_on(4)
    paired(5)
    paired(6)
    pass_on(5)
    partials(7)
    pass_on(6)
    paired(7)
    for m in (5, 6):
        arrived(right_in.at[m], rr_send.at[m], rr_recv.at[m], on_y(1))
        arrived(left_in.at[m], rl_send.at[m], rl_recv.at[m], on_y(NY - 1))
    for half in range(2):
        value = summed(7, half) + right_in[6 - half].astype(F32) + left_in[5 + half].astype(F32)
        back_out[16 * half : 16 * half + 16] = value.reshape(16, CAP, COLS).astype(BF)

    own2 = pltpu.make_async_copy(back_out.at[sp], back_in.at[sp], own_sem.at[1])
    own2.start()

    def back_go(k, carry):
        to = lax.rem(sp + k, SP)
        send(back_out.at[to], back_in.at[sp], b_send.at[k], b_recv.at[k], {"sp": to})
        return carry

    def back_come(k, carry):
        source = lax.rem(sp + SP - k, SP)
        arrived(back_in.at[source], b_send.at[k], b_recv.at[k], {"sp": lax.rem(sp + k, SP)})
        return carry

    lax.fori_loop(1, SP, back_go, 0)
    gain2, shift2 = twice(column(final_gain[...])), twice(column(final_shift[...]))
    lax.fori_loop(1, SP, back_come, 0)
    own2.wait()

    returned = jnp.transpose(back_in[...].astype(F32).reshape(ROWS, COLS)).astype(BF)
    moe = dot(returned, mix_hi[...]) + dot(returned, mix_lo[...])
    second = ALPHA * hid[...] + moe
    center, scale = totals(second, stat2, s2_send, s2_recv)
    out[...] = jnp.transpose((second - center) * scale * gain2 + shift2).astype(BF)

    for i in range(3):
        left_here((tail_k, tail_v, tail_d)[i], tail_sem.at[i], tail_sem.at[3 + i], after)
    for k in range(1, NY):
        left_here(att.at[tp], a_send.at[k], a_recv.at[k], on_y(k))
    for k in range(NY):
        left_here(att.at[tp], as_send.at[k], as_recv.at[k], sibling)

    def stats_left(k, carry):
        left_here(stat1.at[tp], s_send.at[k], s_recv.at[k], {"tp": lax.rem(tp + k, TP)})
        left_here(stat2.at[tp], s2_send.at[k], s2_recv.at[k], {"tp": lax.rem(tp + k, TP)})
        return carry

    def rows_left(k, carry):
        to = lax.rem(sp + k, SP)
        left_here(going.at[to], d_send.at[k], d_recv.at[k], {"sp": to})
        left_here(back_out.at[to], b_send.at[k], b_recv.at[k], {"sp": to})
        return carry

    lax.fori_loop(1, TP, stats_left, 0)
    lax.fori_loop(1, SP, rows_left, 0)
    for m in range(7):
        left_here(grid.at[0, 0], gr_send.at[m], gr_recv.at[m], on_y(1))
        left_here(grid.at[0, 0], gl_send.at[m], gl_recv.at[m], on_y(NY - 1))
        left_here(right_out.at[m], rr_send.at[m], rr_recv.at[m], on_y(1))
        left_here(left_out.at[m], rl_send.at[m], rl_recv.at[m], on_y(NY - 1))
    for index in range(16):
        left_here(grid.at[0, 0], gs_send.at[index], gs_recv.at[index], sibling)
    for i in range(NY):
        left_here(sib_out.at[i], rs_send.at[i], rs_recv.at[i], sibling)


def local(
    residual, queries, keys, values, documents, sinks, head_gain, out_weight, norm_gain, norm_shift,
    routes, route_logits, gate_weight, up_weight, down_weight, final_gain, final_shift,
):
    vmem = pl.BlockSpec(memory_space=pltpu.VMEM)
    smem = pl.BlockSpec(memory_space=pltpu.SMEM)
    hbm = pl.BlockSpec(memory_space=pl.ANY)
    dma = pltpu.SemaphoreType.DMA
    return pl.pallas_call(
        kernel,
        out_shape=jax.ShapeDtypeStruct((TOK, COLS), BF),
        in_specs=[vmem] * 5 + [smem] + [vmem] * 8 + [hbm] * 3,
        out_specs=vmem,
        scratch_shapes=[
            pltpu.VMEM((D, 2 * FFB), BF),
            pltpu.VMEM((NY, FFB, 2 * COLS), BF),
            pltpu.VMEM((WINDOW, 128), BF),
            pltpu.VMEM((WINDOW, 128), BF),
            pltpu.VMEM((1, WINDOW), jnp.int32),
            pltpu.VMEM((COLS, TP * HEAD), BF),
            pltpu.VMEM((COLS, TOK), F32),
            pltpu.VMEM((128, WINDOW + TOK), BF),
            pltpu.VMEM((ROWS, TOK), BF),
            pltpu.VMEM((ROWS, TOK), BF),
            pltpu.VMEM((ROWS, TOK), BF),
            pltpu.VMEM((TP, HEAD, TOK), BF),
            pltpu.VMEM((TP, 2, TOK), F32),
            pltpu.VMEM((TP, 2, TOK), F32),
            pltpu.VMEM((COLS, TOK), F32),
            pltpu.VMEM((SP, CAP, COLS), BF),
            pltpu.VMEM((SP, CAP, COLS), BF),
            pltpu.VMEM((TP, 2, HALF, COLS), BF),
            pltpu.VMEM((2, HALF, 2 * FFB), F32),
            pltpu.VMEM((2, HALF, FFB), BF),
            pltpu.VMEM((NY, 2, HALF, COLS), F32),
            pltpu.VMEM((NY, 2, HALF, COLS), BF),
            pltpu.VMEM((NY, 2, HALF, COLS), BF),
            pltpu.VMEM((7, HALF, COLS), BF),
            pltpu.VMEM((7, HALF, COLS), BF),
            pltpu.VMEM((7, HALF, COLS), BF),
            pltpu.VMEM((7, HALF, COLS), BF),
            pltpu.VMEM((SP, CAP, COLS), BF),
            pltpu.VMEM((SP, CAP, COLS), BF),
            dma((2 + 2 * NY,)),
            dma((6,)),
            dma((NY,)), dma((NY,)), dma((NY,)), dma((NY,)),
            dma((TP,)), dma((TP,)), dma((TP,)), dma((TP,)),
            dma((SP,)), dma((SP,)),
            dma((7,)), dma((7,)), dma((7,)), dma((7,)), dma((16,)), dma((16,)),
            dma((NY,)), dma((NY,)), dma((7,)), dma((7,)), dma((7,)), dma((7,)),
            dma((SP,)), dma((SP,)), dma((2,)),
        ],
        compiler_params=pltpu.CompilerParams(
            collective_id=0, has_side_effects=True, vmem_limit_bytes=60 * 1024 * 1024
        ),
        name="layer",
    )(
        residual, queries.T, keys, values, documents.reshape(1, TOK), sinks.reshape(1, 1),
        head_gain.reshape(1, TP * HEAD), out_weight, norm_gain.reshape(1, COLS), norm_shift.reshape(1, COLS),
        routes.T, route_logits.T, final_gain.reshape(1, COLS), final_shift.reshape(1, COLS),
        gate_weight, up_weight, down_weight,
    )


def solution(mesh):
    return jax.shard_map(
        local,
        mesh=mesh,
        in_specs=(
            P("sp", "tp"), P("sp", "tp"), P("sp", None), P("sp", None), P("sp"), P("tp"), P(), P(None, "tp"),
            P("tp"), P("tp"), P("sp", None), P("sp", None), P("sp", None, "tp"), P("sp", None, "tp"),
            P("sp", "tp", None), P("tp"), P("tp"),
        ),
        out_specs=P("sp", "tp"),
        check_vma=False,
    )
```

time: 269 us -> 105 us (0.39)
  waiting for transfers between devices: 128 us -> 0 us
  Pallas kernels: 0 us -> 102 us
  blocking collectives: 58.5 us -> 0 us
  starting transfers between devices: 28.7 us -> 0 us
  matrix products: 14.8 us -> 0 us
  between operations: 14.4 us -> 0.66 us
  local copies, waits for them, and re-layouts: 15.2 us -> 1.47 us
  other arithmetic: 8.54 us -> 0 us
    pallas_call x0 -> x1, Pallas kernels: none -> 102 us  [local(): pl.pallas_call(kernel, out_shape=jax.ShapeDtypeStruct((TOK, COLS), BF), i...]
    all_to_all x3 -> x0, waiting for transfers between devices: 88.1 us -> none  [the longest x1 71.1 us: expert_rows(): lax.all_to_all(pieces, 'tp', split_axis=2, concat_axis=2, tiled=True)]
    all_gather x1 -> x0, waiting for transfers between devices: 39.9 us -> none  [local(): lax.all_gather(lax.all_to_all(outgoing, 'sp', split_axis=0, concat_axis=0...]
    all_to_all x2 -> x0, blocking collectives: 38.2 us -> none  [the longest x1 23.3 us: local(): lax.all_to_all(outgoing, 'sp', split_axis=0, concat_axis=0, tiled=True)]
    all_gather x1 -> x0, blocking collectives: 20.4 us -> none  [local(): lax.all_gather(attended, 'tp', axis=1, tiled=True).astype(jnp.float32)]
    all_to_all x3 -> x0, starting transfers between devices: 18.8 us -> none  [the longest x1 9.73 us: expert_rows(): lax.all_to_all(summed.astype(jnp.bfloat16), 'sp', split_axis=0, concat_ax...]
    dot_general x5 -> x0, matrix products: 14.8 us -> none  [the longest x1 7.36 us: expert_rows(): jnp.dot(middle, down_weight[0], preferred_element_type=jnp.float32)]
    ppermute x3 -> x0, starting transfers between devices: 9.84 us -> none  [shifted(): return lax.ppermute(block, axis, route)]
  transfers between devices with their start and end apart: 7 -> 0, of which waited for: 4 -> 0; matrix products, arithmetic and copies ran while one was open for 4% -> 0% of each run, Pallas kernels for 0% -> 0%
where the time goes in v1:
time: 105 us; the launch traced here: 104 us
  Pallas kernels  102 us (97%)
  local copies, waits for them, and re-layouts  1.47 us (1%)
    pallas_call x1, Pallas kernels, local(): pl.pallas_call(kernel, out_shape=jax.ShapeDtypeStruct((TOK, COLS), BF), i...  102 us

profile of v1, /device:TPU:1, one launch (start us, length us, event | category | flops | bytes accessed | tf_op | source)
XLA Modules:
  0.0 104.3 jit_solution(15190539032242066177)
XLA Ops:
  0.7 102.2 %layer.1 = bf16[256,128]{1,0:T(8,128)(2,1)} custom-call(bf16[256,128]{1,0:T(8,128)(2,1)} %residual.1, bf16[64,256]{1,0:T(8,128)(2,1)} %bitcast.11, bf16[256,128]{1,0:T(8,128)(2,1)} %keys.1, bf16[256,128]{1,0:T(8,128)(2,1)} %values.1, s32[1,256]{1,0:T(1,128)} %bitcast.15, f32[1,1]{1,0:T(1,128)} %bitcast.10.sinks, f32[1,1024]{1,0:T(1,128)} %bitcast.12, ...), custom_call_target="tpu_custom_call" | custom-call | tf_op jit(solution)/shard_map/layer/pallas_call | solution.py:443
  102.9 1.5 %copy.20 = bf16[256,128]{1,0:T(8,128)(2,1)} copy(bf16[256,128]{1,0:T(8,128)(2,1)} %layer.1) | data formatting | bytes 131072

commit v2 on v1

--- a/solution.py
+++ b/solution.py
@@ -47,13 +47,16 @@
 
 
 def kernel(
+    residual_hbm, queries_hbm, keys_hbm, values_hbm, docs_hbm, sinks_hbm, head_gain_hbm, out_weight_hbm,
+    norm_gain_hbm, norm_shift_hbm, routes_hbm, logits_hbm, final_gain_hbm, final_shift_hbm,
+    gate_hbm, up_hbm, down_hbm,
+    out,
     residual, queries, keys, values, docs, sinks, head_gain, out_weight, norm_gain, norm_shift,
-    routes, logits, final_gain, final_shift, gate_hbm, up_hbm, down_hbm,
-    out,
+    routes, logits, final_gain, final_shift,
     wgu, wd, tail_k, tail_v, tail_d, wot, res, vt, select, mix_hi, mix_lo,
     att, stat1, stat2, hid, going, came, grid, acc, mid, mine, sib_out, sib_in,
     right_out, right_in, left_out, left_in, back_out, back_in,
-    w_sem, tail_sem, a_send, a_recv, as_send, as_recv, s_send, s_recv, s2_send, s2_recv,
+    in_sem, w_sem, tail_sem, a_send, a_recv, as_send, as_recv, s_send, s_recv,
     d_send, d_recv, gr_send, gr_recv, gl_send, gl_recv, gs_send, gs_recv,
     rs_send, rs_recv, rr_send, rr_recv, rl_send, rl_recv, b_send, b_recv, own_sem,
 ):
@@ -87,6 +90,27 @@
             device_id=device, device_id_type=MESH,
         ).wait_send()
 
+    barrier = pltpu.get_barrier_semaphore()
+
+    def greet_tp(k, carry):
+        pl.semaphore_signal(barrier, inc=1, device_id={"tp": lax.rem(tp + k, TP)}, device_id_type=MESH)
+        return carry
+
+    def greet_sp(k, carry):
+        pl.semaphore_signal(barrier, inc=1, device_id={"sp": lax.rem(sp + k, SP)}, device_id_type=MESH)
+        return carry
+
+    lax.fori_loop(1, TP, greet_tp, 0)
+    lax.fori_loop(1, SP, greet_sp, 0)
+    inputs = [
+        (queries_hbm, queries), (keys_hbm, keys), (docs_hbm, docs), (sinks_hbm, sinks), (values_hbm, values),
+        (out_weight_hbm, out_weight), (head_gain_hbm, head_gain), (residual_hbm, residual),
+        (routes_hbm, routes), (logits_hbm, logits), (norm_gain_hbm, norm_gain), (norm_shift_hbm, norm_shift),
+        (final_gain_hbm, final_gain), (final_shift_hbm, final_shift),
+    ]
+    in_copies = [pltpu.make_async_copy(src, dst, in_sem.at[i]) for i, (src, dst) in enumerate(inputs)]
+    for copy in in_copies:
+        copy.start()
     w_copies = [
         pltpu.make_async_copy(gate_hbm.at[0], wgu.at[:, 0:FFB], w_sem.at[0]),
         pltpu.make_async_copy(up_hbm.at[0], wgu.at[:, FFB : 2 * FFB], w_sem.at[1]),
@@ -98,24 +122,13 @@
                 pltpu.make_async_copy(
                     down_hbm.at[0, :, pl.ds(pl.multiple_of(block * 128, 128), 128)],
                     wd.at[d, :, 128 * part : 128 * part + 128],
-                    w_sem.at[2 + 2 * d + part],
+                    w_sem.at[2],
                 )
             )
     for copy in w_copies:
         copy.start()
-
-    barrier = pltpu.get_barrier_semaphore()
-
-    def greet_tp(k, carry):
-        pl.semaphore_signal(barrier, inc=1, device_id={"tp": lax.rem(tp + k, TP)}, device_id_type=MESH)
-        return carry
-
-    def greet_sp(k, carry):
-        pl.semaphore_signal(barrier, inc=1, device_id={"sp": lax.rem(sp + k, SP)}, device_id_type=MESH)
-        return carry
-
-    lax.fori_loop(1, TP, greet_tp, 0)
-    lax.fori_loop(1, SP, greet_sp, 0)
+    for copy in in_copies[:5]:
+        copy.wait()
 
     upper = tp >= TP // 2
     vt[:, WINDOW:] = jnp.transpose(values[...].astype(F32)).astype(BF)
@@ -123,7 +136,7 @@
     zero_q = jnp.zeros_like(qt)
     q_wide = jnp.concatenate([jnp.where(upper, zero_q, qt), jnp.where(upper, qt, zero_q)], axis=0)
     doc_row = docs[...].astype(F32)
-    sink = sinks[0, 0]
+    sink = sinks[...]
 
     def attend(key_rows, v_cols, key_docs, begin):
         score = dot(key_rows, q_wide[:, begin : begin + 128]) * HEAD ** (-0.5)
@@ -143,7 +156,7 @@
 
     docs0 = column(doc_row[:, 0:128])
     docs1 = column(doc_row[:, 128:256])
-    att[tp, :, 128:256] = attend(keys[...], vt[:, 128:384], jnp.concatenate([docs0, docs1], axis=0), 128)
+    att[1, y, c] = attend(keys[...], vt[:, 128:384], jnp.concatenate([docs0, docs1], axis=0), 128)
 
     pl.semaphore_wait(barrier, TP - 1 + SP - 1)
 
@@ -152,6 +165,14 @@
     send(values.at[128:256], tail_v, tail_sem.at[1], tail_sem.at[4], after)
     send(docs.at[:, 128:256], tail_d, tail_sem.at[2], tail_sem.at[5], after)
 
+    def heads_go(block):
+        for k in (4, 3, 5, 2, 6, 1, 7):
+            send(att.at[block, y, c], att.at[block, y, c], a_send.at[block], a_recv.at[block], on_y(k))
+
+    heads_go(1)
+
+    for copy in in_copies[5:]:
+        copy.wait()
     wot[...] = (jnp.transpose(out_weight[...].astype(F32)) * head_gain[...]).astype(BF)
     res[...] = ALPHA * jnp.transpose(residual[...].astype(F32))
 
@@ -160,16 +181,14 @@
     arrived(tail_d, tail_sem.at[2], tail_sem.at[5], after)
     vt[:, 0:WINDOW] = jnp.transpose(tail_v[...].astype(F32)).astype(BF)
     before_docs = jnp.where(sp > 0, tail_d[...].astype(F32), -1.0)
-    att[tp, :, 0:128] = attend(
+    att[0, y, c] = attend(
         jnp.concatenate([tail_k[...], keys[0:128, :]], axis=0),
         vt[:, 0:256],
         jnp.concatenate([column(before_docs), docs0], axis=0),
         0,
     )
 
-    send(att.at[tp], att.at[tp], as_send.at[0], as_recv.at[0], sibling)
-    for k in (4, 3, 5, 2, 6, 1, 7):
-        send(att.at[tp], att.at[tp], a_send.at[k], a_recv.at[k], on_y(k))
+    heads_go(0)
 
     r0, r1 = routes[0:1, :], routes[1:2, :]
     experts = lax.broadcasted_iota(jnp.int32, (SP, TOK), 0)
@@ -199,17 +218,17 @@
         mix_lo[rows, :] = (weight - high.astype(F32)).astype(BF)
     gain1, shift1 = twice(column(norm_gain[...])), twice(column(norm_shift[...]))
 
-    for k in (1, 7, 2, 6, 3, 5, 4):
-        block = att.at[chip(NY - k) * 2 + c]
-        arrived(block, a_send.at[k], a_recv.at[k], on_y(k))
-        send(block, block, as_send.at[k], as_recv.at[k], sibling)
-    for k in range(NY):
-        arrived(att.at[chip(NY - k) * 2 + 1 - c], as_send.at[k], as_recv.at[k], sibling)
-
-    heads = att[...].reshape(TP * HEAD, TOK)
-    wide = heads.astype(F32)
-    scale = lax.rsqrt(jnp.sum(wide * wide, axis=0, keepdims=True) * (1.0 / (TP * HEAD)) + EPS)
-    first = res[...] + dot(wot[...], heads) * scale
+    for block in (1, 0):
+        arrived(att.at[block, 0:7, c], a_send.at[block], a_recv.at[block], on_y(1))
+        send(att.at[block, :, c], att.at[block, :, c], as_send.at[block], as_recv.at[block], sibling)
+    first = []
+    for block in (1, 0):
+        arrived(att.at[block, :, 1 - c], as_send.at[block], as_recv.at[block], sibling)
+        heads = att[block].reshape(TP * HEAD, 128)
+        wide = heads.astype(F32)
+        scale = lax.rsqrt(jnp.sum(wide * wide, axis=0, keepdims=True) * (1.0 / (TP * HEAD)) + EPS)
+        first.append(res[:, 128 * block : 128 * block + 128] + dot(wot[...], heads) * scale)
+    first = jnp.concatenate([first[1], first[0]], axis=1)
 
     def totals(value, stat, send_sem, recv_sem):
         stat[tp] = jnp.concatenate(
@@ -217,21 +236,17 @@
         )
 
         def tell(k, carry):
-            send(stat.at[tp], stat.at[tp], send_sem.at[k], recv_sem.at[k], {"tp": lax.rem(tp + k, TP)})
+            send(stat.at[tp], stat.at[tp], send_sem, recv_sem, {"tp": lax.rem(tp + k, TP)})
             return carry
 
-        def hear(k, carry):
-            arrived(stat.at[lax.rem(tp + TP - k, TP)], send_sem.at[k], recv_sem.at[k], {"tp": lax.rem(tp + k, TP)})
-            return carry
-
         lax.fori_loop(1, TP, tell, 0)
-        lax.fori_loop(1, TP, hear, 0)
+        arrived(stat.at[0 : TP - 1], send_sem, recv_sem, sibling)
         total = jnp.sum(stat[...], axis=0)
         center = total[0:1] * (1.0 / D)
         spread = total[1:2] * (1.0 / D) - center * center
         return center, lax.rsqrt(spread + EPS)
 
-    center, scale = totals(first, stat1, s_send, s_recv)
+    center, scale = totals(first, stat1, s_send.at[0], s_recv.at[0])
     hidden = (first - center) * scale * gain1 + shift1
     hid[...] = hidden
 
@@ -242,18 +257,13 @@
 
     def out_go(k, carry):
         to = lax.rem(sp + k, SP)
-        send(going.at[to], came.at[sp], d_send.at[k], d_recv.at[k], {"sp": to})
-        return carry
-
-    def out_come(k, carry):
-        source = lax.rem(sp + SP - k, SP)
-        arrived(came.at[source], d_send.at[k], d_recv.at[k], {"sp": lax.rem(sp + k, SP)})
+        send(going.at[to], came.at[sp], d_send.at[0], d_recv.at[0], {"sp": to})
         return carry
 
     lax.fori_loop(1, SP, out_go, 0)
     w_copies[0].wait()
     w_copies[1].wait()
-    lax.fori_loop(1, SP, out_come, 0)
+    arrived(came.at[0 : SP - 1], d_send.at[0], d_recv.at[0], after)
     own.wait()
 
     for half in range(2):
@@ -267,13 +277,13 @@
         hops, half = lanes[m]
         if lanes is RIGHT:
             p = piece(NY - hops, half, c)
-            send(p, p, gr_send.at[m], gr_recv.at[m], on_y(1))
+            send(p, p, gr_send.at[0], gr_recv.at[m], on_y(1))
         else:
             p = piece(hops, half, c)
-            send(p, p, gl_send.at[m], gl_recv.at[m], on_y(NY - 1))
+            send(p, p, gl_send.at[0], gl_recv.at[m], on_y(NY - 1))
 
     def share_send(index, p):
-        send(p, p, gs_send.at[index], gs_recv.at[index], sibling)
+        send(p, p, gs_send.at[0], gs_recv.at[index], sibling)
 
     for m in range(2):
         ring_send(m, RIGHT)
@@ -291,7 +301,7 @@
             acc[half] += product
 
     for half in range(2):
-        arrived(piece(0, half, 1 - c), gs_send.at[half], gs_recv.at[half], sibling)
+        arrived(piece(0, half, 1 - c), gs_send.at[0], gs_recv.at[half], sibling)
         multiply(0, half, True)
     waiting = []
     for m in range(7):
@@ -302,21 +312,20 @@
             owner = NY - 1 - hops if right else hops + 1
             p = piece(owner, half, c)
             s, r = (gr_send, gr_recv) if right else (gl_send, gl_recv)
-            arrived(p, s.at[m], r.at[m], on_y(1 if right else NY - 1))
+            arrived(p, s.at[0], r.at[m], on_y(1 if right else NY - 1))
             if m + 2 < 7:
                 ring_send(m + 2, lanes)
             index = 2 + 2 * m + (0 if right else 1)
             share_send(index, p)
             now.append((owner, half, index))
         for owner, half, index in waiting:
-            arrived(piece(owner, half, 1 - c), gs_send.at[index], gs_recv.at[index], sibling)
+            arrived(piece(owner, half, 1 - c), gs_send.at[0], gs_recv.at[index], sibling)
             multiply(owner, half, False)
         waiting = now
     for owner, half, index in waiting:
-        arrived(piece(owner, half, 1 - c), gs_send.at[index], gs_recv.at[index], sibling)
+        arrived(piece(owner, half, 1 - c), gs_send.at[0], gs_recv.at[index], sibling)
         multiply(owner, half, False)
-    for copy in w_copies[2:]:
-        copy.wait()
+    pltpu.make_async_copy(wd, wd, w_sem.at[2]).wait()
     for half in range(2):
         gate, up = acc[half, :, 0:FFB], acc[half, :, FFB:]
         mid[half] = (gate / (1.0 + jnp.exp(-gate)) * up).astype(BF)
@@ -326,10 +335,10 @@
             product = dot(mid[half], wd[chip(DESTS[i])])
             mine[i, half] = product[:, 0:COLS]
             sib_out[i, half] = product[:, COLS:].astype(BF)
-        send(sib_out.at[i], sib_in.at[i], rs_send.at[i], rs_recv.at[i], sibling)
+        send(sib_out.at[i], sib_in.at[i], rs_send.at[0], rs_recv.at[i], sibling)
 
     def paired(i):
-        arrived(sib_in.at[i], rs_send.at[i], rs_recv.at[i], sibling)
+        arrived(sib_in.at[i], rs_send.at[0], rs_recv.at[i], sibling)
 
     def summed(i, half):
         return mine[i, half] + sib_in[i, half].astype(F32)
@@ -342,10 +351,10 @@
             i, half = lanes[m]
             value = summed(i, half)
             if m >= 2:
-                arrived(n.at[m - 2], s.at[m - 2], r.at[m - 2], on_y(d))
+                arrived(n.at[m - 2], s.at[0], r.at[m - 2], on_y(d))
                 value = value + n[m - 2].astype(F32)
             o[m] = value.astype(BF)
-            send(o.at[m], n.at[m], s.at[m], r.at[m], on_y(d))
+            send(o.at[m], n.at[m], s.at[0], r.at[m], on_y(d))
 
     partials(0)
     partials(1)
@@ -371,8 +380,8 @@
     pass_on(6)
     paired(7)
     for m in (5, 6):
-        arrived(right_in.at[m], rr_send.at[m], rr_recv.at[m], on_y(1))
-        arrived(left_in.at[m], rl_send.at[m], rl_recv.at[m], on_y(NY - 1))
+        arrived(right_in.at[m], rr_send.at[0], rr_recv.at[m], on_y(1))
+        arrived(left_in.at[m], rl_send.at[0], rl_recv.at[m], on_y(NY - 1))
     for half in range(2):
         value = summed(7, half) + right_in[6 - half].astype(F32) + left_in[5 + half].astype(F32)
         back_out[16 * half : 16 * half + 16] = value.reshape(16, CAP, COLS).astype(BF)
@@ -382,54 +391,34 @@
 
     def back_go(k, carry):
         to = lax.rem(sp + k, SP)
-        send(back_out.at[to], back_in.at[sp], b_send.at[k], b_recv.at[k], {"sp": to})
-        return carry
-
-    def back_come(k, carry):
-        source = lax.rem(sp + SP - k, SP)
-        arrived(back_in.at[source], b_send.at[k], b_recv.at[k], {"sp": lax.rem(sp + k, SP)})
+        send(back_out.at[to], back_in.at[sp], b_send.at[0], b_recv.at[0], {"sp": to})
         return carry
 
     lax.fori_loop(1, SP, back_go, 0)
     gain2, shift2 = twice(column(final_gain[...])), twice(column(final_shift[...]))
-    lax.fori_loop(1, SP, back_come, 0)
+    arrived(back_in.at[0 : SP - 1], b_send.at[0], b_recv.at[0], after)
     own2.wait()
 
     returned = jnp.transpose(back_in[...].astype(F32).reshape(ROWS, COLS)).astype(BF)
     moe = dot(returned, mix_hi[...]) + dot(returned, mix_lo[...])
     second = ALPHA * hid[...] + moe
-    center, scale = totals(second, stat2, s2_send, s2_recv)
+    center, scale = totals(second, stat2, s_send.at[1], s_recv.at[1])
     out[...] = jnp.transpose((second - center) * scale * gain2 + shift2).astype(BF)
 
     for i in range(3):
         left_here((tail_k, tail_v, tail_d)[i], tail_sem.at[i], tail_sem.at[3 + i], after)
-    for k in range(1, NY):
-        left_here(att.at[tp], a_send.at[k], a_recv.at[k], on_y(k))
-    for k in range(NY):
-        left_here(att.at[tp], as_send.at[k], as_recv.at[k], sibling)
-
-    def stats_left(k, carry):
-        left_here(stat1.at[tp], s_send.at[k], s_recv.at[k], {"tp": lax.rem(tp + k, TP)})
-        left_here(stat2.at[tp], s2_send.at[k], s2_recv.at[k], {"tp": lax.rem(tp + k, TP)})
-        return carry
-
-    def rows_left(k, carry):
-        to = lax.rem(sp + k, SP)
-        left_here(going.at[to], d_send.at[k], d_recv.at[k], {"sp": to})
-        left_here(back_out.at[to], b_send.at[k], b_recv.at[k], {"sp": to})
-        return carry
-
-    lax.fori_loop(1, TP, stats_left, 0)
-    lax.fori_loop(1, SP, rows_left, 0)
-    for m in range(7):
-        left_here(grid.at[0, 0], gr_send.at[m], gr_recv.at[m], on_y(1))
-        left_here(grid.at[0, 0], gl_send.at[m], gl_recv.at[m], on_y(NY - 1))
-        left_here(right_out.at[m], rr_send.at[m], rr_recv.at[m], on_y(1))
-        left_here(left_out.at[m], rl_send.at[m], rl_recv.at[m], on_y(NY - 1))
-    for index in range(16):
-        left_here(grid.at[0, 0], gs_send.at[index], gs_recv.at[index], sibling)
-    for i in range(NY):
-        left_here(sib_out.at[i], rs_send.at[i], rs_recv.at[i], sibling)
+    for block in range(2):
+        left_here(att.at[block, 0:7, 0], a_send.at[block], a_recv.at[block], on_y(1))
+        left_here(att.at[block, :, 0], as_send.at[block], as_recv.at[block], sibling)
+        left_here(stat1.at[0 : TP - 1], s_send.at[block], s_recv.at[block], sibling)
+    left_here(going.at[0 : SP - 1], d_send.at[0], d_recv.at[0], after)
+    left_here(back_out.at[0 : SP - 1], b_send.at[0], b_recv.at[0], after)
+    left_here(right_out, gr_send.at[0], gr_recv.at[0], on_y(1))
+    left_here(left_out, gl_send.at[0], gl_recv.at[0], on_y(NY - 1))
+    left_here(right_out, rr_send.at[0], rr_recv.at[0], on_y(1))
+    left_here(left_out, rl_send.at[0], rl_recv.at[0], on_y(NY - 1))
+    left_here(sib_out, gs_send.at[0], gs_recv.at[0], sibling)
+    left_here(sib_out, rs_send.at[0], rs_recv.at[0], sibling)
 
 
 def local(
@@ -437,15 +426,28 @@
     routes, route_logits, gate_weight, up_weight, down_weight, final_gain, final_shift,
 ):
     vmem = pl.BlockSpec(memory_space=pltpu.VMEM)
-    smem = pl.BlockSpec(memory_space=pltpu.SMEM)
     hbm = pl.BlockSpec(memory_space=pl.ANY)
     dma = pltpu.SemaphoreType.DMA
     return pl.pallas_call(
         kernel,
-        out_shape=jax.ShapeDtypeStruct((TOK, COLS), BF),
-        in_specs=[vmem] * 5 + [smem] + [vmem] * 8 + [hbm] * 3,
+        out_shape=pltpu.VMEM((TOK, COLS), BF),
+        in_specs=[hbm] * 17,
         out_specs=vmem,
         scratch_shapes=[
+            pltpu.VMEM((TOK, COLS), BF),
+            pltpu.VMEM((HEAD, TOK), BF),
+            pltpu.VMEM((TOK, 128), BF),
+            pltpu.VMEM((TOK, 128), BF),
+            pltpu.VMEM((1, TOK), jnp.int32),
+            pltpu.VMEM((1, 1), F32),
+            pltpu.VMEM((1, TP * HEAD), F32),
+            pltpu.VMEM((TP * HEAD, COLS), BF),
+            pltpu.VMEM((1, COLS), F32),
+            pltpu.VMEM((1, COLS), F32),
+            pltpu.VMEM((2, TOK), jnp.int32),
+            pltpu.VMEM((2, TOK), F32),
+            pltpu.VMEM((1, COLS), F32),
+            pltpu.VMEM((1, COLS), F32),
             pltpu.VMEM((D, 2 * FFB), BF),
             pltpu.VMEM((NY, FFB, 2 * COLS), BF),
             pltpu.VMEM((WINDOW, 128), BF),
@@ -457,7 +459,7 @@
             pltpu.VMEM((ROWS, TOK), BF),
             pltpu.VMEM((ROWS, TOK), BF),
             pltpu.VMEM((ROWS, TOK), BF),
-            pltpu.VMEM((TP, HEAD, TOK), BF),
+            pltpu.VMEM((2, NY, 2, HEAD, 128), BF),
             pltpu.VMEM((TP, 2, TOK), F32),
             pltpu.VMEM((TP, 2, TOK), F32),
             pltpu.VMEM((COLS, TOK), F32),
@@ -475,14 +477,12 @@
             pltpu.VMEM((7, HALF, COLS), BF),
             pltpu.VMEM((SP, CAP, COLS), BF),
             pltpu.VMEM((SP, CAP, COLS), BF),
-            dma((2 + 2 * NY,)),
-            dma((6,)),
-            dma((NY,)), dma((NY,)), dma((NY,)), dma((NY,)),
-            dma((TP,)), dma((TP,)), dma((TP,)), dma((TP,)),
-            dma((SP,)), dma((SP,)),
-            dma((7,)), dma((7,)), dma((7,)), dma((7,)), dma((16,)), dma((16,)),
-            dma((NY,)), dma((NY,)), dma((7,)), dma((7,)), dma((7,)), dma((7,)),
-            dma((SP,)), dma((SP,)), dma((2,)),
+            dma((14,)), dma((3,)), dma((6,)),
+            dma((2,)), dma((2,)), dma((2,)), dma((2,)), dma((2,)), dma((2,)),
+            dma((1,)), dma((1,)),
+            dma((1,)), dma((7,)), dma((1,)), dma((7,)), dma((1,)), dma((16,)),
+            dma((1,)), dma((NY,)), dma((1,)), dma((7,)), dma((1,)), dma((7,)),
+            dma((1,)), dma((1,)), dma((2,)),
         ],
         compiler_params=pltpu.CompilerParams(
             collective_id=0, has_side_effects=True, vmem_limit_bytes=60 * 1024 * 1024

time: 105 us -> 95.7 us (0.911)
  Pallas kernels: 102 us -> 94.3 us
    pallas_call x1, Pallas kernels: 102 us -> 94.3 us  [local(): pl.pallas_call(kernel, out_shape=pltpu.VMEM((TOK, COLS), BF), in_specs=[h...]
where the time goes in v2:
time: 95.7 us; the launch traced here: 95.6 us
  Pallas kernels  94.3 us (99%)
    pallas_call x1, Pallas kernels, local(): pl.pallas_call(kernel, out_shape=pltpu.VMEM((TOK, COLS), BF), in_specs=[h...  94.3 us

profile of v2, /device:TPU:1, one launch (start us, length us, event | category | flops | bytes accessed | tf_op | source)
XLA Modules:
  0.0 95.6 jit_solution(14491089334865092467)
XLA Ops:
  0.7 94.3 %layer.1 = bf16[256,128]{1,0:T(8,128)(2,1)S(1)} custom-call(bf16[256,128]{1,0:T(8,128)(2,1)} %residual_hbm.1, bf16[64,256]{1,0:T(8,128)(2,1)} %bitcast.11, bf16[256,128]{1,0:T(8,128)(2,1)} %keys_hbm.1, bf16[256,128]{1,0:T(8,128)(2,1)} %values_hbm.1, s32[1,256]{1,0:T(1,128)} %bitcast.15, f32[1,1]{1,0:T(1,128)} %bitcast.10.sinks_hbm, f32[1,1024]{1,0:T(1,128)} %bitcast.12, ...), custom_call_target="tpu_custom_call" | custom-call | tf_op jit(solution)/shard_map/layer/pallas_call | solution.py:431
  95.0 0.6 copy.19

commit v3 on v2

--- a/solution.py
+++ b/solution.py
@@ -23,11 +23,30 @@
 BF = jnp.bfloat16
 F32 = jnp.float32
 
-RIGHT = [(0, 0), (0, 1), (1, 0), (1, 1), (2, 0), (2, 1), (3, 0)]
-LEFT = [(0, 1), (0, 0), (1, 1), (1, 0), (2, 1), (2, 0), (3, 1)]
+QUARTER = ROWS // 4
+PLACES = sorted(
+    [(dz, dx) for dz in range(8) for dx in range(4)], key=lambda p: min(p[0], 8 - p[0]) + min(p[1], 4 - p[1])
+)
+
+
+def gather_order(near, near_too, far, far_too):
+    return [
+        (0, near), (0, near_too), (1, near), (1, near_too), (0, far), (0, far_too), (2, near), (2, near_too),
+        (1, far), (1, far_too), (3, near), (2, far), (2, far_too), (3, far),
+    ]
+
+
+def sum_order(near, near_too, far, far_too):
+    return [
+        (4, near), (3, near_too), (3, near), (4, far), (3, far_too), (2, near_too), (3, far), (2, near),
+        (2, far_too), (2, far), (1, near_too), (1, far_too), (1, far), (1, near),
+    ]
+
+
+RIGHT, LEFT = gather_order(0, 1, 2, 3), gather_order(1, 0, 3, 2)
+SUM_RIGHT, SUM_LEFT = sum_order(0, 1, 2, 3), sum_order(1, 0, 3, 2)
+MESSAGES = len(RIGHT)
 DESTS = [4, 3, 5, 2, 6, 1, 7, 0]
-SUM_RIGHT = [(0, 0), (1, 1), (1, 0), (3, 1), (3, 0), (5, 1), (5, 0)]
-SUM_LEFT = [(0, 1), (2, 0), (2, 1), (4, 0), (4, 1), (6, 0), (6, 1)]
 
 
 def dot(a, b):
@@ -53,10 +72,10 @@
     out,
     residual, queries, keys, values, docs, sinks, head_gain, out_weight, norm_gain, norm_shift,
     routes, logits, final_gain, final_shift,
-    wgu, wd, tail_k, tail_v, tail_d, wot, res, vt, select, mix_hi, mix_lo,
-    att, stat1, stat2, hid, going, came, grid, acc, mid, mine, sib_out, sib_in,
+    wgu, wd, tail_k, tail_v, tail_d, wot, res, vt, select, mix_hi, mix_lo, facts, rows_gu,
+    att, stat1, stat2, hid, going, came, grid, acc, acc1, acc2, mid, mine, sib_out, sib_in,
     right_out, right_in, left_out, left_in, back_out, back_in,
-    in_sem, w_sem, tail_sem, a_send, a_recv, as_send, as_recv, s_send, s_recv,
+    in_sem, w_sem, tail_sem, f_send, f_recv, a_send, a_recv, as_send, as_recv, s_send, s_recv,
     d_send, d_recv, gr_send, gr_recv, gl_send, gl_recv, gs_send, gs_recv,
     rs_send, rs_recv, rr_send, rr_recv, rl_send, rl_recv, b_send, b_recv, own_sem,
 ):
@@ -64,6 +83,8 @@
     tp = lax.axis_index("tp")
     y = lax.div(tp, 2)
     c = lax.rem(tp, 2)
+    z = lax.div(sp, 4)
+    x = lax.rem(sp, 4)
     sibling = {"tp": y * 2 + 1 - c}
 
     def chip(distance):
@@ -92,16 +113,6 @@
 
     barrier = pltpu.get_barrier_semaphore()
 
-    def greet_tp(k, carry):
-        pl.semaphore_signal(barrier, inc=1, device_id={"tp": lax.rem(tp + k, TP)}, device_id_type=MESH)
-        return carry
-
-    def greet_sp(k, carry):
-        pl.semaphore_signal(barrier, inc=1, device_id={"sp": lax.rem(sp + k, SP)}, device_id_type=MESH)
-        return carry
-
-    lax.fori_loop(1, TP, greet_tp, 0)
-    lax.fori_loop(1, SP, greet_sp, 0)
     inputs = [
         (queries_hbm, queries), (keys_hbm, keys), (docs_hbm, docs), (sinks_hbm, sinks), (values_hbm, values),
         (out_weight_hbm, out_weight), (head_gain_hbm, head_gain), (residual_hbm, residual),
@@ -109,7 +120,20 @@
         (final_gain_hbm, final_gain), (final_shift_hbm, final_shift),
     ]
     in_copies = [pltpu.make_async_copy(src, dst, in_sem.at[i]) for i, (src, dst) in enumerate(inputs)]
-    for copy in in_copies:
+    for copy in in_copies[:5]:
+        copy.start()
+
+    def greet_tp(k, carry):
+        pl.semaphore_signal(barrier, inc=1, device_id={"tp": lax.rem(tp + k, TP)}, device_id_type=MESH)
+        return carry
+
+    def greet_sp(k, carry):
+        pl.semaphore_signal(barrier, inc=1, device_id={"sp": lax.rem(sp + k, SP)}, device_id_type=MESH)
+        return carry
+
+    lax.fori_loop(1, TP, greet_tp, 0)
+    lax.fori_loop(1, SP, greet_sp, 0)
+    for copy in in_copies[5:]:
         copy.start()
     w_copies = [
         pltpu.make_async_copy(gate_hbm.at[0], wgu.at[:, 0:FFB], w_sem.at[0]),
@@ -125,10 +149,10 @@
                     w_sem.at[2],
                 )
             )
+    for copy in in_copies[:5]:
+        copy.wait()
     for copy in w_copies:
         copy.start()
-    for copy in in_copies[:5]:
-        copy.wait()
 
     upper = tp >= TP // 2
     vt[:, WINDOW:] = jnp.transpose(values[...].astype(F32)).astype(BF)
@@ -175,6 +199,15 @@
         copy.wait()
     wot[...] = (jnp.transpose(out_weight[...].astype(F32)) * head_gain[...]).astype(BF)
     res[...] = ALPHA * jnp.transpose(residual[...].astype(F32))
+    over = jnp.sum(wot[...].astype(F32), axis=0, keepdims=True)
+    res_sum = jnp.sum(res[...], axis=0, keepdims=True)
+    facts[y, c] = jnp.concatenate(
+        [norm_gain[...], norm_shift[...], res_sum[:, 0:128], res_sum[:, 128:256]]
+        + [over[:, 128 * i : 128 * i + 128] for i in range(8)],
+        axis=0,
+    )
+    for k in (4, 3, 5, 2, 6, 1, 7):
+        send(facts.at[y, c], facts.at[y, c], f_send.at[0], f_recv.at[0], on_y(k))
 
     arrived(tail_k, tail_sem.at[0], tail_sem.at[3], after)
     arrived(tail_v, tail_sem.at[1], tail_sem.at[4], after)
@@ -218,183 +251,266 @@
         mix_lo[rows, :] = (weight - high.astype(F32)).astype(BF)
     gain1, shift1 = twice(column(norm_gain[...])), twice(column(norm_shift[...]))
 
+    arrived(facts.at[0:7, c], f_send.at[0], f_recv.at[0], on_y(1))
+    send(facts.at[:, c], facts.at[:, c], f_send.at[1], f_recv.at[1], sibling)
+    arrived(att.at[1, 0:7, c], a_send.at[1], a_recv.at[1], on_y(1))
+    send(att.at[1, :, c], att.at[1, :, c], as_send.at[1], as_recv.at[1], sibling)
+    arrived(facts.at[:, 1 - c], f_send.at[1], f_recv.at[1], sibling)
+
+    fact = jnp.sum(facts[...].reshape(TP, 12, 128), axis=0) * (1.0 / D)
+    over = jnp.concatenate([fact[4 + i : 5 + i] for i in range(8)], axis=1)
+    over = jnp.broadcast_to(over, (8, TP * HEAD)).astype(BF)
+
+    firsts, centred = [], []
     for block in (1, 0):
-        arrived(att.at[block, 0:7, c], a_send.at[block], a_recv.at[block], on_y(1))
-        send(att.at[block, :, c], att.at[block, :, c], as_send.at[block], as_recv.at[block], sibling)
-    first = []
-    for block in (1, 0):
+        if block == 0:
+            arrived(att.at[0, 0:7, c], a_send.at[0], a_recv.at[0], on_y(1))
+            send(att.at[0, :, c], att.at[0, :, c], as_send.at[0], as_recv.at[0], sibling)
         arrived(att.at[block, :, 1 - c], as_send.at[block], as_recv.at[block], sibling)
         heads = att[block].reshape(TP * HEAD, 128)
         wide = heads.astype(F32)
         scale = lax.rsqrt(jnp.sum(wide * wide, axis=0, keepdims=True) * (1.0 / (TP * HEAD)) + EPS)
-        first.append(res[:, 128 * block : 128 * block + 128] + dot(wot[...], heads) * scale)
-    first = jnp.concatenate([first[1], first[0]], axis=1)
-
-    def totals(value, stat, send_sem, recv_sem):
+        value = res[:, 128 * block : 128 * block + 128] + dot(wot[...], heads) * scale
+        middle = fact[2 + block : 3 + block] + dot(over, heads)[0:1] * scale
+        firsts.append(value)
+        centred.append((value - middle).astype(BF))
+    first = jnp.concatenate([firsts[1], firsts[0]], axis=1)
+    centred = jnp.concatenate([centred[1], centred[0]], axis=1)
+    hid[...] = first
+
+    def tell(value, stat, send_sem, recv_sem):
         stat[tp] = jnp.concatenate(
             [jnp.sum(value, axis=0, keepdims=True), jnp.sum(value * value, axis=0, keepdims=True)], axis=0
         )
 
-        def tell(k, carry):
+        def one(k, carry):
             send(stat.at[tp], stat.at[tp], send_sem, recv_sem, {"tp": lax.rem(tp + k, TP)})
             return carry
 
-        lax.fori_loop(1, TP, tell, 0)
+        lax.fori_loop(1, TP, one, 0)
+
+    def hear(stat, send_sem, recv_sem):
         arrived(stat.at[0 : TP - 1], send_sem, recv_sem, sibling)
         total = jnp.sum(stat[...], axis=0)
         center = total[0:1] * (1.0 / D)
         spread = total[1:2] * (1.0 / D) - center * center
         return center, lax.rsqrt(spread + EPS)
 
-    center, scale = totals(first, stat1, s_send.at[0], s_recv.at[0])
-    hidden = (first - center) * scale * gain1 + shift1
-    hid[...] = hidden
-
-    packed = dot_nt(select[...], hidden.astype(BF))
+    packed = dot_nt(select[...], centred)
     going[...] = packed.reshape(SP, CAP, COLS).astype(BF)
-    own = pltpu.make_async_copy(going.at[sp], came.at[sp], own_sem.at[0])
+    own = pltpu.make_async_copy(going.at[sp], came.at[0], own_sem.at[0])
     own.start()
-
-    def out_go(k, carry):
-        to = lax.rem(sp + k, SP)
-        send(going.at[to], came.at[sp], d_send.at[0], d_recv.at[0], {"sp": to})
-        return carry
-
-    lax.fori_loop(1, SP, out_go, 0)
+    for k in range(1, SP):
+        to = lax.rem(z + 8 - PLACES[k][0], 8) * 4 + lax.rem(x + 4 - PLACES[k][1], 4)
+        send(going.at[to], came.at[k], d_send.at[0], d_recv.at[k // 16], {"sp": to})
+    tell(first, stat1, s_send.at[0], s_recv.at[0])
+
     w_copies[0].wait()
     w_copies[1].wait()
-    arrived(came.at[0 : SP - 1], d_send.at[0], d_recv.at[0], after)
-    own.wait()
-
-    for half in range(2):
-        block = came[16 * half : 16 * half + 16].astype(F32).reshape(HALF, COLS)
-        grid[tp, half] = block.astype(BF)
-
-    def piece(owner, half, core):
-        return grid.at[chip(owner) * 2 + core, half]
+
+    def fold(i, carry):
+        sums, shifts = carry
+        at = pl.ds(pl.multiple_of(i * 128, 128), 128)
+        fact = facts[lax.div(i, 2), lax.rem(i, 2)]
+        gain_wide, shift_wide = column(fact[0:1]), column(fact[1:2])
+        new_sums, new_shifts = [], []
+        for j in range(6):
+            lanes = slice(128 * j, 128 * j + 128)
+            weight = wgu[at, lanes].astype(F32)
+            gained = (weight * gain_wide).astype(BF)
+            wgu[at, lanes] = gained
+            new_sums.append(jnp.sum(gained.astype(F32), axis=0, keepdims=True))
+            new_shifts.append(jnp.sum(weight * shift_wide, axis=0, keepdims=True))
+        return sums + jnp.concatenate(new_sums, axis=1), shifts + jnp.concatenate(new_shifts, axis=1)
+
+    none = jnp.zeros((1, 2 * FFB), F32)
+    w_sums, w_shifts = lax.fori_loop(0, TP, fold, (none, none))
+    rows_gu[0:1, :] = w_sums
+    rows_gu[1:2, :] = w_shifts
+
+    def piece(owner, quarter, core):
+        return grid.at[chip(owner) * 2 + core, quarter]
 
     def ring_send(m, lanes):
-        hops, half = lanes[m]
+        hops, quarter = lanes[m]
         if lanes is RIGHT:
-            p = piece(NY - hops, half, c)
+            p = piece(NY - hops, quarter, c)
             send(p, p, gr_send.at[0], gr_recv.at[m], on_y(1))
         else:
-            p = piece(hops, half, c)
+            p = piece(hops, quarter, c)
             send(p, p, gl_send.at[0], gl_recv.at[m], on_y(NY - 1))
 
-    def share_send(index, p):
-        send(p, p, gs_send.at[0], gs_recv.at[index], sibling)
-
-    for m in range(2):
-        ring_send(m, RIGHT)
-        ring_send(m, LEFT)
-    for half in range(2):
-        share_send(half, piece(0, half, c))
-
-    def multiply(owner, half, fresh):
+    def begin(half):
+        block = came[16 * half : 16 * half + 16].astype(F32).reshape(HALF, COLS).astype(BF)
+        grid[tp, 2 * half] = block[:QUARTER]
+        grid[tp, 2 * half + 1] = block[QUARTER:]
+        for m in (4 * half, 4 * half + 1):
+            ring_send(m, RIGHT)
+            ring_send(m, LEFT)
+        p = grid.at[tp, 2 * half : 2 * half + 2]
+        send(p, p, gs_send.at[0], gs_recv.at[half], sibling)
+
+    def ring_take(m):
+        for lanes in (RIGHT, LEFT):
+            hops, quarter = lanes[m]
+            right = lanes is RIGHT
+            owner = NY - 1 - hops if right else hops + 1
+            p = piece(owner, quarter, c)
+            s, r = (gr_send, gr_recv) if right else (gl_send, gl_recv)
+            arrived(p, s.at[0], r.at[m], on_y(1 if right else NY - 1))
+            if (hops + 1, quarter) in lanes:
+                ring_send(lanes.index((hops + 1, quarter)), lanes)
+            send(p, p, gs_send.at[0], gs_recv.at[2 * owner + quarter // 2], sibling)
+
+    def multiply(owner, half):
         at = chip(owner)
-        both = jnp.concatenate([grid[at * 2, half], grid[at * 2 + 1, half]], axis=1)
-        product = dot(both, wgu[pl.ds(pl.multiple_of(at * 256, 256), 256), :])
-        if fresh:
+        rows = slice(2 * half, 2 * half + 2)
+        arrived(grid.at[at * 2 + 1 - c, rows], gs_send.at[0], gs_recv.at[2 * owner + half], sibling)
+        one, two = grid[at * 2, rows].reshape(HALF, COLS), grid[at * 2 + 1, rows].reshape(HALF, COLS)
+        product = dot(jnp.concatenate([one, two], axis=1), wgu[pl.ds(pl.multiple_of(at * 256, 256), 256), :])
+        one, two = one.astype(F32), two.astype(F32)
+        if owner == 0:
             acc[half] = product
+            acc1[half] = one + two
+            acc2[half] = one * one + two * two
         else:
             acc[half] += product
-
-    for half in range(2):
-        arrived(piece(0, half, 1 - c), gs_send.at[0], gs_recv.at[half], sibling)
-        multiply(0, half, True)
-    waiting = []
-    for m in range(7):
-        now = []
-        for lanes in (RIGHT, LEFT):
-            hops, half = lanes[m]
-            right = lanes is RIGHT
-            owner = NY - 1 - hops if right else hops + 1
-            p = piece(owner, half, c)
-            s, r = (gr_send, gr_recv) if right else (gl_send, gl_recv)
-            arrived(p, s.at[0], r.at[m], on_y(1 if right else NY - 1))
-            if m + 2 < 7:
-                ring_send(m + 2, lanes)
-            index = 2 + 2 * m + (0 if right else 1)
-            share_send(index, p)
-            now.append((owner, half, index))
-        for owner, half, index in waiting:
-            arrived(piece(owner, half, 1 - c), gs_send.at[0], gs_recv.at[index], sibling)
-            multiply(owner, half, False)
-        waiting = now
-    for owner, half, index in waiting:
-        arrived(piece(owner, half, 1 - c), gs_send.at[0], gs_recv.at[index], sibling)
-        multiply(owner, half, False)
+            acc1[half] += one + two
+            acc2[half] += one * one + two * two
+
+    def activate(half):
+        center = jnp.sum(acc1[half], axis=1, keepdims=True) * (1.0 / D)
+        spread = jnp.sum(acc2[half], axis=1, keepdims=True) * (1.0 / D) - center * center
+        scale = lax.rsqrt(spread + EPS)
+        gate = (acc[half, :, 0:FFB] - center * rows_gu[0:1, 0:FFB]) * scale + rows_gu[1:2, 0:FFB]
+        up = (acc[half, :, FFB:] - center * rows_gu[0:1, FFB:]) * scale + rows_gu[1:2, FFB:]
+        mid[half] = (gate / (1.0 + jnp.exp(-gate)) * up).astype(BF)
+
+    arrived(came.at[1:16], d_send.at[0], d_recv.at[0], after)
+    own.wait()
+    begin(0)
+    multiply(0, 0)
+    ring_take(0)
+    ring_take(1)
+    arrived(came.at[16:32], d_send.at[0], d_recv.at[1], after)
+    begin(1)
+    multiply(1, 0)
+    multiply(7, 0)
+    ring_take(2)
+    multiply(0, 1)
+    ring_take(3)
+    center, scale = hear(stat1, s_send.at[0], s_recv.at[0])
+    hid[...] = (hid[...] - center) * scale * gain1 + shift1
+    ring_take(4)
+    multiply(2, 0)
+    ring_take(5)
+    multiply(6, 0)
+    ring_take(6)
+    multiply(1, 1)
+    ring_take(7)
+    multiply(7, 1)
+    ring_take(8)
+    multiply(3, 0)
+    ring_take(9)
+    multiply(5, 0)
+    ring_take(10)
+    multiply(2, 1)
+    ring_take(11)
+    multiply(4, 0)
+    activate(0)
+
     pltpu.make_async_copy(wd, wd, w_sem.at[2]).wait()
-    for half in range(2):
-        gate, up = acc[half, :, 0:FFB], acc[half, :, FFB:]
-        mid[half] = (gate / (1.0 + jnp.exp(-gate)) * up).astype(BF)
-
-    def partials(i):
-        for half in range(2):
-            product = dot(mid[half], wd[chip(DESTS[i])])
-            mine[i, half] = product[:, 0:COLS]
-            sib_out[i, half] = product[:, COLS:].astype(BF)
-        send(sib_out.at[i], sib_in.at[i], rs_send.at[0], rs_recv.at[i], sibling)
-
-    def paired(i):
-        arrived(sib_in.at[i], rs_send.at[0], rs_recv.at[i], sibling)
-
-    def summed(i, half):
-        return mine[i, half] + sib_in[i, half].astype(F32)
+    waited = set()
+
+    def partials(i, half):
+        rows = slice(2 * half, 2 * half + 2)
+        product = dot(mid[half], wd[chip(DESTS[i])])
+        mine[i, rows] = product[:, 0:COLS].reshape(2, QUARTER, COLS)
+        sib_out[i, rows] = product[:, COLS:].astype(BF).reshape(2, QUARTER, COLS)
+        send(sib_out.at[i, rows], sib_in.at[i, rows], rs_send.at[0], rs_recv.at[2 * i + half], sibling)
+
+    def summed(i, quarter):
+        half = quarter // 2
+        if (i, half) not in waited:
+            waited.add((i, half))
+            rows = slice(2 * half, 2 * half + 2)
+            arrived(sib_in.at[i, rows], rs_send.at[0], rs_recv.at[2 * i + half], sibling)
+        return mine[i, quarter] + sib_in[i, quarter].astype(F32)
+
+    def passed(lanes, hops, quarter):
+        m = lanes.index((hops, quarter))
+        if lanes is SUM_RIGHT:
+            arrived(right_in.at[m], rr_send.at[0], rr_recv.at[m], on_y(1))
+            return right_in[m].astype(F32)
+        arrived(left_in.at[m], rl_send.at[0], rl_recv.at[m], on_y(NY - 1))
+        return left_in[m].astype(F32)
 
     def pass_on(m):
-        for lanes, o, n, s, r, d in (
-            (SUM_RIGHT, right_out, right_in, rr_send, rr_recv, 1),
-            (SUM_LEFT, left_out, left_in, rl_send, rl_recv, NY - 1),
-        ):
-            i, half = lanes[m]
-            value = summed(i, half)
-            if m >= 2:
-                arrived(n.at[m - 2], s.at[0], r.at[m - 2], on_y(d))
-                value = value + n[m - 2].astype(F32)
-            o[m] = value.astype(BF)
-            send(o.at[m], n.at[m], s.at[0], r.at[m], on_y(d))
-
-    partials(0)
-    partials(1)
-    partials(2)
-    paired(0)
+        for lanes in (SUM_RIGHT, SUM_LEFT):
+            hops, quarter = lanes[m]
+            right = lanes is SUM_RIGHT
+            value = summed(DESTS.index(hops if right else NY - hops), quarter)
+            if (hops + 1, quarter) in lanes:
+                value = value + passed(lanes, hops + 1, quarter)
+            if right:
+                right_out[m] = value.astype(BF)
+                send(right_out.at[m], right_in.at[m], rr_send.at[0], rr_recv.at[m], on_y(1))
+            else:
+                left_out[m] = value.astype(BF)
+                send(left_out.at[m], left_in.at[m], rl_send.at[0], rl_recv.at[m], on_y(NY - 1))
+
+    partials(0, 0)
+    partials(1, 0)
+    partials(2, 0)
+    ring_take(12)
+    multiply(6, 1)
     pass_on(0)
-    paired(1)
-    paired(2)
     pass_on(1)
-    partials(3)
-    partials(4)
+    multiply(3, 1)
+    multiply(5, 1)
+    ring_take(13)
+    multiply(4, 1)
+    activate(1)
+    partials(0, 1)
+    partials(1, 1)
+    partials(2, 1)
     pass_on(2)
-    paired(3)
-    paired(4)
     pass_on(3)
-    partials(5)
-    partials(6)
     pass_on(4)
-    paired(5)
-    paired(6)
+    partials(3, 0)
+    partials(4, 0)
+    partials(3, 1)
+    partials(4, 1)
     pass_on(5)
-    partials(7)
     pass_on(6)
-    paired(7)
-    for m in (5, 6):
-        arrived(right_in.at[m], rr_send.at[0], rr_recv.at[m], on_y(1))
-        arrived(left_in.at[m], rl_send.at[0], rl_recv.at[m], on_y(NY - 1))
-    for half in range(2):
-        value = summed(7, half) + right_in[6 - half].astype(F32) + left_in[5 + half].astype(F32)
+    partials(5, 0)
+    partials(6, 0)
+    pass_on(7)
+    pass_on(8)
+    partials(5, 1)
+    partials(6, 1)
+    pass_on(9)
+    partials(7, 1)
+    partials(7, 0)
+    pass_on(10)
+    pass_on(11)
+    pass_on(12)
+    pass_on(13)
+
+    def back_go(half):
+        values = [
+            summed(7, q) + passed(SUM_RIGHT, 1, q) + passed(SUM_LEFT, 1, q) for q in (2 * half, 2 * half + 1)
+        ]
+        value = jnp.concatenate(values, axis=0)
         back_out[16 * half : 16 * half + 16] = value.reshape(16, CAP, COLS).astype(BF)
-
-    own2 = pltpu.make_async_copy(back_out.at[sp], back_in.at[sp], own_sem.at[1])
+        for k in range(max(1, 16 * half), 16 * half + 16):
+            to = lax.rem(z + PLACES[k][0], 8) * 4 + lax.rem(x + PLACES[k][1], 4)
+            send(back_out.at[k], back_in.at[sp], b_send.at[0], b_recv.at[0], {"sp": to})
+
+    back_go(1)
+    back_go(0)
+    own2 = pltpu.make_async_copy(back_out.at[0], back_in.at[sp], own_sem.at[1])
     own2.start()
-
-    def back_go(k, carry):
-        to = lax.rem(sp + k, SP)
-        send(back_out.at[to], back_in.at[sp], b_send.at[0], b_recv.at[0], {"sp": to})
-        return carry
-
-    lax.fori_loop(1, SP, back_go, 0)
     gain2, shift2 = twice(column(final_gain[...])), twice(column(final_shift[...]))
     arrived(back_in.at[0 : SP - 1], b_send.at[0], b_recv.at[0], after)
     own2.wait()
@@ -402,7 +518,8 @@
     returned = jnp.transpose(back_in[...].astype(F32).reshape(ROWS, COLS)).astype(BF)
     moe = dot(returned, mix_hi[...]) + dot(returned, mix_lo[...])
     second = ALPHA * hid[...] + moe
-    center, scale = totals(second, stat2, s_send.at[1], s_recv.at[1])
+    tell(second, stat2, s_send.at[1], s_recv.at[1])
+    center, scale = hear(stat2, s_send.at[1], s_recv.at[1])
     out[...] = jnp.transpose((second - center) * scale * gain2 + shift2).astype(BF)
 
     for i in range(3):
@@ -411,6 +528,8 @@
         left_here(att.at[block, 0:7, 0], a_send.at[block], a_recv.at[block], on_y(1))
         left_here(att.at[block, :, 0], as_send.at[block], as_recv.at[block], sibling)
         left_here(stat1.at[0 : TP - 1], s_send.at[block], s_recv.at[block], sibling)
+    left_here(facts.at[0:7, 0], f_send.at[0], f_recv.at[0], on_y(1))
+    left_here(facts.at[:, 0], f_send.at[1], f_recv.at[1], sibling)
     left_here(going.at[0 : SP - 1], d_send.at[0], d_recv.at[0], after)
     left_here(back_out.at[0 : SP - 1], b_send.at[0], b_recv.at[0], after)
     left_here(right_out, gr_send.at[0], gr_recv.at[0], on_y(1))
@@ -459,29 +578,33 @@
             pltpu.VMEM((ROWS, TOK), BF),
             pltpu.VMEM((ROWS, TOK), BF),
             pltpu.VMEM((ROWS, TOK), BF),
+            pltpu.VMEM((NY, 2, 12, 128), F32),
+            pltpu.VMEM((2, 2 * FFB), F32),
             pltpu.VMEM((2, NY, 2, HEAD, 128), BF),
             pltpu.VMEM((TP, 2, TOK), F32),
             pltpu.VMEM((TP, 2, TOK), F32),
             pltpu.VMEM((COLS, TOK), F32),
             pltpu.VMEM((SP, CAP, COLS), BF),
             pltpu.VMEM((SP, CAP, COLS), BF),
-            pltpu.VMEM((TP, 2, HALF, COLS), BF),
+            pltpu.VMEM((TP, 4, QUARTER, COLS), BF),
             pltpu.VMEM((2, HALF, 2 * FFB), F32),
+            pltpu.VMEM((2, HALF, COLS), F32),
+            pltpu.VMEM((2, HALF, COLS), F32),
             pltpu.VMEM((2, HALF, FFB), BF),
-            pltpu.VMEM((NY, 2, HALF, COLS), F32),
-            pltpu.VMEM((NY, 2, HALF, COLS), BF),
-            pltpu.VMEM((NY, 2, HALF, COLS), BF),
-            pltpu.VMEM((7, HALF, COLS), BF),
-            pltpu.VMEM((7, HALF, COLS), BF),
-            pltpu.VMEM((7, HALF, COLS), BF),
-            pltpu.VMEM((7, HALF, COLS), BF),
+            pltpu.VMEM((NY, 4, QUARTER, COLS), F32),
+            pltpu.VMEM((NY, 4, QUARTER, COLS), BF),
+            pltpu.VMEM((NY, 4, QUARTER, COLS), BF),
+            pltpu.VMEM((MESSAGES, QUARTER, COLS), BF),
+            pltpu.VMEM((MESSAGES, QUARTER, COLS), BF),
+            pltpu.VMEM((MESSAGES, QUARTER, COLS), BF),
+            pltpu.VMEM((MESSAGES, QUARTER, COLS), BF),
             pltpu.VMEM((SP, CAP, COLS), BF),
             pltpu.VMEM((SP, CAP, COLS), BF),
             dma((14,)), dma((3,)), dma((6,)),
-            dma((2,)), dma((2,)), dma((2,)), dma((2,)), dma((2,)), dma((2,)),
-            dma((1,)), dma((1,)),
-            dma((1,)), dma((7,)), dma((1,)), dma((7,)), dma((1,)), dma((16,)),
-            dma((1,)), dma((NY,)), dma((1,)), dma((7,)), dma((1,)), dma((7,)),
+            dma((2,)), dma((2,)), dma((2,)), dma((2,)), dma((2,)), dma((2,)), dma((2,)), dma((2,)),
+            dma((1,)), dma((2,)),
+            dma((1,)), dma((MESSAGES,)), dma((1,)), dma((MESSAGES,)), dma((1,)), dma((2 * NY,)),
+            dma((1,)), dma((2 * NY,)), dma((1,)), dma((MESSAGES,)), dma((1,)), dma((MESSAGES,)),
             dma((1,)), dma((1,)), dma((2,)),
         ],
         compiler_params=pltpu.CompilerParams(

time: 95.7 us -> 87.6 us (0.915)
  Pallas kernels: 94.3 us -> 86.1 us
    pallas_call x1, Pallas kernels: 94.3 us -> 86.1 us  [local(): pl.pallas_call(kernel, out_shape=pltpu.VMEM((TOK, COLS), BF), in_specs=[h...]
where the time goes in v3:
time: 87.6 us; the launch traced here: 87.4 us
  Pallas kernels  86.1 us (98%)
    pallas_call x1, Pallas kernels, local(): pl.pallas_call(kernel, out_shape=pltpu.VMEM((TOK, COLS), BF), in_specs=[h...  86.1 us

profile of v3, /device:TPU:1, one launch (start us, length us, event | category | flops | bytes accessed | tf_op | source)
XLA Modules:
  0.0 87.4 jit_solution(150273356524009786)
XLA Ops:
  0.7 86.1 %layer.1 = bf16[256,128]{1,0:T(8,128)(2,1)S(1)} custom-call(bf16[256,128]{1,0:T(8,128)(2,1)} %residual_hbm.1, bf16[64,256]{1,0:T(8,128)(2,1)} %bitcast.11, bf16[256,128]{1,0:T(8,128)(2,1)} %keys_hbm.1, bf16[256,128]{1,0:T(8,128)(2,1)} %values_hbm.1, s32[1,256]{1,0:T(1,128)} %bitcast.15, f32[1,1]{1,0:T(1,128)} %bitcast.10.sinks_hbm, f32[1,1024]{1,0:T(1,128)} %bitcast.12, ...), custom_call_target="tpu_custom_call" | custom-call | tf_op jit(solution)/shard_map/layer/pallas_call | solution.py:550
  86.8 0.6 copy.19
